TPU v7x, 128 devices: a whole 4x4x4 slice. The times are simulated.
128 devices in a mesh: sp: 16 (over z, y), tp: 8 (over x, core).
Axes of the slice: x: 4, y: 4, z: 4, core: 2. Of those that a mesh axis runs over, the one named last changes fastest.
Arguments:
- inputs: bfloat16 [16384, 2048], P('sp'), may hold values from -6 to 6
- norm_gain: float32 [3, 2048], replicated, may hold values from 0.1 to 1.9
- query_weight: bfloat16 [3, 2048, 1024], P(None, 'sp', 'tp'), may hold values from -64 to 64
- key_weight: bfloat16 [3, 2048, 512], P(None, 'sp', 'tp'), may hold values from -4 to 4
- value_weight: bfloat16 [3, 2048, 512], P(None, 'sp', 'tp'), may hold values from -0.125 to 0.125
- output_weight: bfloat16 [3, 2048, 1024], P(None, 'sp', 'tp'), may hold values from -0.1875 to 0.1875
- sink_logit: float32 [3, 16], P(None, 'tp'), may hold values from 2 to 7
- final_gain: float32 [2048], replicated, may hold values from 0.1 to 1.9
Outputs:
- result: float32 [16384, 2048], P(('sp', 'tp'))
All inputs are finite; a program needn't handle non-finite values.
Results may differ from a plain program's by a relative error of at most 0.015.
Values may be sent and summed in bfloat16 or wider, within the bound.
A program may use at most 64 MiB of HBM per device.

v0:
```python
import jax
import jax.numpy as jnp
from jax import lax
from jax.sharding import PartitionSpec as P

D = 2048
HEAD_DIM = 64
WINDOW = 128
LAYERS = 3


EPS = 1e-06


def sent_together(arrays, axis, dim, along):
    both = jnp.concatenate(arrays, axis=along)
    result, at, done = (lax.all_gather(both, axis, axis=dim, tiled=True), 0, [])
    for a in arrays:
        done.append(lax.slice_in_dim(result, at, at + a.shape[along], axis=along))
        at += a.shape[along]
    return tuple(done)


def extended_2(block, sides, width):
    for axis, dim in sides:
        count = lax.axis_size(axis)
        forward = [(i, i + 1) for i in range(count - 1)]
        backward = [(target, source) for source, target in forward]
        low = lax.ppermute(
            lax.slice_in_dim(block, block.shape[dim] - width, None, axis=dim), axis, forward
        )
        high = lax.ppermute(lax.slice_in_dim(block, 0, width, axis=dim), axis, backward)
        block = jnp.concatenate([low, block, high], axis=dim)
    return block


def norm_rows(values, gain):
    wide_values = values.astype(jnp.float32)
    inv_root = lax.rsqrt(jnp.mean(wide_values * wide_values, axis=-1, keepdims=True) + EPS)
    return wide_values * inv_root * gain


def rotate(values, places):
    half_dim = values.shape[-1] // 2
    inverse = 10000.0 ** (-jnp.arange(half_dim).astype(jnp.float32) / half_dim)
    angles = places[:, None] * inverse[None, :]
    cosine_table = jnp.cos(angles)[:, None, :]
    sine_table = jnp.sin(angles)[:, None, :]
    front_half = values[..., :half_dim]
    back_half = values[..., half_dim:]
    return jnp.concatenate(
        [
            front_half * cosine_table - back_half * sine_table,
            back_half * cosine_table + front_half * sine_table,
        ],
        axis=-1,
    )


def attend(queries, key_rows, value_rows, sink_row, allowed):
    scores = jnp.einsum(
        "qkgd,skd->kgqs", queries, key_rows, preferred_element_type=jnp.float32
    ) * queries.shape[-1] ** (-0.5)
    scores = jnp.where(allowed[None, None], scores, -jnp.inf)
    sink_col = sink_row[:, :, None]
    largest = jnp.maximum(jnp.max(scores, axis=-1), sink_col)
    powers = jnp.exp(scores - largest[..., None])
    denominator = jnp.sum(powers, axis=-1) + jnp.exp(sink_col - largest)
    weights = (powers / denominator[..., None]).astype(jnp.bfloat16)
    blended = jnp.einsum("kgqs,skd->qkgd", weights, value_rows, preferred_element_type=jnp.float32)
    return blended.astype(jnp.bfloat16)


def shards(
    inputs, norm_gain, query_weight, key_weight, value_weight, output_weight, sink_logit, final_gain
):
    tokens = inputs.shape[0]
    local_heads = query_weight.shape[2] // HEAD_DIM
    local_groups = key_weight.shape[2] // HEAD_DIM
    per_group = local_heads // local_groups
    kv_cols = local_groups * HEAD_DIM
    offset = lax.axis_index("sp") * tokens
    seq_total = tokens * lax.axis_size("sp")
    query_pos = offset + jnp.arange(tokens, dtype=jnp.int32)
    places = query_pos.astype(jnp.float32)
    key_pos = offset - WINDOW + jnp.arange(tokens + 2 * WINDOW, dtype=jnp.int32)
    allowed = (
        (jnp.abs(key_pos[None, :] - query_pos[:, None]) <= WINDOW)
        & (key_pos[None, :] >= 0)
        & (key_pos[None, :] < seq_total)
    )
    whole_query, whole_key, whole_value, whole_out = sent_together(
        (query_weight, key_weight, value_weight, output_weight), "sp", 1, 2
    )
    current = inputs
    final_rows = inputs
    for layer in range(LAYERS):
        normed = norm_rows(current, norm_gain[layer]).astype(jnp.bfloat16)
        query_raw = jnp.dot(normed, whole_query[layer], preferred_element_type=jnp.float32)
        key_raw = jnp.dot(normed, whole_key[layer], preferred_element_type=jnp.float32)
        value_raw = jnp.dot(normed, whole_value[layer], preferred_element_type=jnp.float32)
        out_weight = whole_out[layer]
        queries = rotate(
            (query_raw * float(D) ** (-0.5)).reshape(tokens, local_heads, HEAD_DIM), places
        ).astype(jnp.bfloat16)
        key_rot = rotate(
            (key_raw * float(D) ** (-0.5)).reshape(tokens, local_groups, HEAD_DIM), places
        ).astype(jnp.bfloat16)
        packed = jnp.concatenate(
            [key_rot.reshape(tokens, kv_cols), value_raw.astype(jnp.bfloat16)], axis=1
        )
        extended = extended_2(packed, (("sp", 0),), WINDOW)
        key_rows = extended[:, :kv_cols].reshape(-1, local_groups, HEAD_DIM)
        value_all = extended[:, kv_cols:].reshape(-1, local_groups, HEAD_DIM)
        sink_row = sink_logit[layer].reshape(local_groups, per_group)
        attended = attend(
            queries.reshape(tokens, local_groups, per_group, HEAD_DIM),
            key_rows,
            value_all,
            sink_row,
            allowed,
        )
        attended = attended.reshape(tokens, local_heads * HEAD_DIM)

        def project():
            return lax.dot_general(
                attended, out_weight, (((1,), (1,)), ((), ())), preferred_element_type=jnp.float32
            )

        if layer < LAYERS - 1:
            share_rows = lax.psum_scatter(project(), "tp", scatter_dimension=0, tiled=True).astype(
                jnp.bfloat16
            )
            current = lax.all_gather(share_rows, "tp", axis=0, tiled=True)
        else:
            final_rows = lax.psum_scatter(
                project().astype(jnp.bfloat16), "tp", scatter_dimension=0, tiled=True
            )
    return norm_rows(final_rows, final_gain)


def solution(mesh):
    in_specs = (
        P("sp", None),
        P(),
        P(None, "sp", "tp"),
        P(None, "sp", "tp"),
        P(None, "sp", "tp"),
        P(None, "sp", "tp"),
        P(None, "tp"),
        P(),
    )
    out_specs = P(("sp", "tp"), None)
    return jax.shard_map(shards, mesh=mesh, in_specs=in_specs, out_specs=out_specs, check_vma=False)
```

profile of v0, /device:TPU:0, one launch (start us, length us, event | category | flops | bytes accessed | tf_op | source)
XLA Modules:
  0.0 389.7 jit_solution(7353681811122570966)
XLA Ops:
  8.4 1.8 pad_maximum_fusion.3
  10.3 1.1 slice_reduce_fusion
  11.4 3.2 fusion.3
  15.2 3.0 fusion.5
  18.2 2.2 fusion.22
  20.4 46.3 %all-gather.4.cloned.1.call-done = bf16[3,2048,384]{2,1,0:T(8,128)(2,1)} async-done(((bf16[3,128,384]{2,1,0:T(8,128)(2,1)}), bf16[3,2048,384]{2,1,0:T(8,128)(2,1)}) %all-gather.4.cloned.1.call-update) | async-done | bytes 4718608 | tf_op jit(solution)/shard_map/all_gather | solution.py:17
  66.8 3.8 fusion.34
  71.2 2.5 convolution_convert_fusion.3
  73.7 3.4 collective-permute-start
  77.1 1.5 collective-permute-start.1
  78.6 2.6 convolution_multiply_fusion.2
  81.3 1.7 collective-permute-done.1
  83.0 2.2 fusion.12
  85.3 2.5 fusion
  87.9 3.5 fusion.23
  91.4 5.6 %fusion.38 = f32[1024,2048]{1,0:T(8,128)} fusion(bf16[1024,128]{0,1:T(8,128)(2,1)S(1)} %bitcast.174, bf16[3,2048,384]{2,1,0:T(8,128)(2,1)} %all-gather.4.cloned.1.call-done), kind=kOutput, calls=%fused_computation.69 | convolution fusion | flops 536870912 | bytes 9175040 | tf_op jit(solution)/shard_map/dot_general | solution.py:126
  97.0 55.1 %reduce-scatter.4.cloned.1.call-done = f32[128,2048]{1,0:T(8,128)} async-done(((f32[1024,2048]{1,0:T(8,128)}), f32[128,2048]{1,0:T(8,128)}) %reduce-scatter.4.cloned.1.call-update) | async-done | bytes 1048592 | tf_op jit(solution)/shard_map/reduce_scatter | solution.py:131
  152.2 2.1 convert_element_type.126
  154.5 31.5 %all-gather.6.cloned.1.call-done = bf16[1024,2048]{1,0:T(8,128)(2,1)} async-done(((bf16[128,2048]{1,0:T(8,128)(2,1)}), bf16[1024,2048]{1,0:T(8,128)(2,1)}) %all-gather.6.cloned.1.call-update) | async-done | bytes 4194320 | tf_op jit(solution)/shard_map/all_gather | solution.py:134
  186.1 3.2 fusion.6
  189.5 1.0 fusion.8
  190.5 2.5 fusion.33
  193.6 2.5 convolution_convert_fusion.2
  196.1 3.4 collective-permute-start.2
  199.5 1.3 collective-permute-start.3
  200.8 2.6 convolution_multiply_fusion.1
  203.5 1.8 collective-permute-done.3
  205.3 2.2 fusion.13
  207.7 2.5 fusion.1
  210.2 3.5 fusion.26
  213.8 5.6 %fusion.37 = f32[1024,2048]{1,0:T(8,128)} fusion(bf16[1024,128]{0,1:T(8,128)(2,1)S(1)} %bitcast.175, bf16[3,2048,384]{2,1,0:T(8,128)(2,1)} %all-gather.4.cloned.1.call-done), kind=kOutput, calls=%fused_computation.64 | convolution fusion | flops 536870912 | bytes 9175040 | tf_op jit(solution)/shard_map/dot_general | solution.py:126
  219.4 54.0 %reduce-scatter.6.cloned.1.call-done = f32[128,2048]{1,0:T(8,128)} async-done(((f32[1024,2048]{1,0:T(8,128)}), f32[128,2048]{1,0:T(8,128)}) %reduce-scatter.6.cloned.1.call-update) | async-done | bytes 1048592 | tf_op jit(solution)/shard_map/reduce_scatter | solution.py:131
  273.4 2.1 convert_element_type.134
  275.9 31.5 %all-gather.8.cloned.1.call-done = bf16[1024,2048]{1,0:T(8,128)(2,1)} async-done(((bf16[128,2048]{1,0:T(8,128)(2,1)}), bf16[1024,2048]{1,0:T(8,128)(2,1)}) %all-gather.8.cloned.1.call-update) | async-done | bytes 4194320 | tf_op jit(solution)/shard_map/all_gather | solution.py:134
  307.3 3.2 fusion.9
  311.8 2.4 fusion.32
  314.8 2.5 convolution_convert_fusion.1
  317.4 3.4 collective-permute-start.4
  320.8 1.3 collective-permute-start.5
  322.1 2.6 convolution_multiply_fusion
  324.7 1.8 collective-permute-done.5
  326.6 2.2 fusion.14
  328.9 2.5 fusion.2
  331.5 3.5 fusion.29
  335.0 4.3 %convolution_convert_fusion = bf16[1024,2048]{1,0:T(8,128)(2,1)} fusion(bf16[1024,128]{0,1:T(8,128)(2,1)S(1)} %bitcast.176, bf16[3,2048,384]{2,1,0:T(8,128)(2,1)} %all-gather.4.cloned.1.call-done), kind=kOutput, calls=%fused_computation.39 | convolution fusion | flops 538968064 | bytes 4980736 | tf_op jit(solution)/shard_map/dot_general | solution.py:126
  339.3 39.6 %reduce-scatter.8.cloned.1.call-done = bf16[128,2048]{1,0:T(8,128)(2,1)} async-done(((bf16[1024,2048]{1,0:T(8,128)(2,1)}), bf16[128,2048]{1,0:T(8,128)(2,1)}) %reduce-scatter.8.cloned.1.call-update) | async-done | bytes 524304 | tf_op jit(solution)/shard_map/reduce_scatter | solution.py:136
  378.9 1.2 fusion.35
  380.2 2.2 fusion.36
  (59 shorter events, 7.2 us)
Async XLA Ops:
  6.5 8.7 %copy-start.4 = (f32[3,2048]{1,0:T(4,128)S(1)}, f32[3,2048]{1,0:T(4,128)}, u32[]{:S(2)}) copy-start(f32[3,2048]{1,0:T(4,128)} %param.9) | copy-start | bytes 73732
  6.5 60.2 %all-gather.4.cloned.1.call-start = ((), (), s32[]{:S(2)}) async-start(), calls=%async_computation.3 | async-start | bytes 5013504 | tf_op jit(solution)/shard_map/all_gather | solution.py:17
  10.2 142.0 %reduce-scatter.4.cloned.1.call-start = ((), (), s32[]{:S(2)}) async-start(), calls=%async_computation.4 | async-start | bytes 9437184 | tf_op jit(solution)/shard_map/reduce_scatter | solution.py:131
  10.3 5.0 %copy-start.1 = (bf16[1024,2048]{1,0:T(8,128)(2,1)S(1)}, bf16[1024,2048]{1,0:T(8,128)(2,1)}, u32[]{:S(2)}) copy-start(bf16[1024,2048]{1,0:T(8,128)(2,1)} %param.8) | copy-start | bytes 12582916
  66.8 4.4 %copy-start = (bf16[1024,2048]{1,0:T(8,128)(2,1)S(1)}, bf16[1024,2048]{1,0:T(8,128)(2,1)}, u32[]{:S(2)}) copy-start(bf16[1024,2048]{1,0:T(8,128)(2,1)} %fusion.5) | copy-start | bytes 12582916
  73.7 7.5 %collective-permute-start = (bf16[128,128]{0,1:T(8,128)(2,1)S(1)}, bf16[128,128]{0,1:T(8,128)(2,1)S(1)}, u32[]{:S(2)}, u32[]{:S(2)}) collective-permute-start(bf16[128,128]{0,1:T(8,128)(2,1)S(1)} %get-tuple-element.24), channel_id=1, source_target_pairs={{0,8},{8,16},{16,24},{24,32},{32,40},{40,48},{48,56},{56,64},{64,7... | collective-permute-start | bytes 98312 | tf_op jit(solution)/shard_map/ppermute | solution.py:29
  77.1 5.8 %collective-permute-start.1 = (bf16[128,128]{0,1:T(8,128)(2,1)S(1)}, bf16[128,128]{0,1:T(8,128)(2,1)S(1)}, u32[]{:S(2)}, u32[]{:S(2)}) collective-permute-start(bf16[128,128]{0,1:T(8,128)(2,1)S(1)} %get-tuple-element.25), channel_id=1, source_target_pairs={{8,0},{16,8},{24,16},{32,24},{40,32},{48,40},{56,48},{64,56},{72,6... | collective-permute-start | bytes 98312 | tf_op jit(solution)/shard_map/ppermute | solution.py:32
  97.0 89.1 %all-gather.6.cloned.1.call-start = ((), (), s32[]{:S(2)}) async-start(), calls=%async_computation.5 | async-start | bytes 4718592 | tf_op jit(solution)/shard_map/all_gather | solution.py:134
  154.3 119.2 %reduce-scatter.6.cloned.1.call-start = ((), (), s32[]{:S(2)}) async-start(), calls=%async_computation.6 | async-start | bytes 9437184 | tf_op jit(solution)/shard_map/reduce_scatter | solution.py:131
  186.1 3.4 copy-start.3
  196.1 7.4 %collective-permute-start.2 = (bf16[128,128]{0,1:T(8,128)(2,1)S(1)}, bf16[128,128]{0,1:T(8,128)(2,1)S(1)}, u32[]{:S(2)}, u32[]{:S(2)}) collective-permute-start(bf16[128,128]{0,1:T(8,128)(2,1)S(1)} %get-tuple-element.22), channel_id=1, source_target_pairs={{0,8},{8,16},{16,24},{24,32},{32,40},{40,48},{48,56},{56,64},{64,7... | collective-permute-start | bytes 98312 | tf_op jit(solution)/shard_map/ppermute | solution.py:29
  199.5 5.8 %collective-permute-start.3 = (bf16[128,128]{0,1:T(8,128)(2,1)S(1)}, bf16[128,128]{0,1:T(8,128)(2,1)S(1)}, u32[]{:S(2)}, u32[]{:S(2)}) collective-permute-start(bf16[128,128]{0,1:T(8,128)(2,1)S(1)} %get-tuple-element.23), channel_id=1, source_target_pairs={{8,0},{16,8},{24,16},{32,24},{40,32},{48,40},{56,48},{64,56},{72,6... | collective-permute-start | bytes 98312 | tf_op jit(solution)/shard_map/ppermute | solution.py:32
  219.4 88.0 %all-gather.8.cloned.1.call-start = ((), (), s32[]{:S(2)}) async-start(), calls=%async_computation.7 | async-start | bytes 4718592 | tf_op jit(solution)/shard_map/all_gather | solution.py:134
  275.6 103.4 %reduce-scatter.8.cloned.1.call-start = ((), (), s32[]{:S(2)}) async-start(), calls=%async_computation.8 | async-start | bytes 4718592 | tf_op jit(solution)/shard_map/reduce_scatter | solution.py:136
  307.3 3.4 copy-start.2
  317.4 7.4 %collective-permute-start.4 = (bf16[128,128]{0,1:T(8,128)(2,1)S(1)}, bf16[128,128]{0,1:T(8,128)(2,1)S(1)}, u32[]{:S(2)}, u32[]{:S(2)}) collective-permute-start(bf16[128,128]{0,1:T(8,128)(2,1)S(1)} %get-tuple-element.20), channel_id=1, source_target_pairs={{0,8},{8,16},{16,24},{24,32},{32,40},{40,48},{48,56},{56,64},{64,7... | collective-permute-start | bytes 98312 | tf_op jit(solution)/shard_map/ppermute | solution.py:29
  320.8 5.8 %collective-permute-start.5 = (bf16[128,128]{0,1:T(8,128)(2,1)S(1)}, bf16[128,128]{0,1:T(8,128)(2,1)S(1)}, u32[]{:S(2)}, u32[]{:S(2)}) collective-permute-start(bf16[128,128]{0,1:T(8,128)(2,1)S(1)} %get-tuple-element.21), channel_id=1, source_target_pairs={{8,0},{16,8},{24,16},{32,24},{40,32},{48,40},{56,48},{64,56},{72,6... | collective-permute-start | bytes 98312 | tf_op jit(solution)/shard_map/ppermute | solution.py:32
  335.0 45.1 %copy-start.5 = (f32[2048]{0:T(1024)S(1)}, f32[2048]{0:T(1024)}, u32[]{:S(2)}) copy-start(f32[2048]{0:T(1024)} %param.15) | copy-start | bytes 24580
Sparse Core Ops, SparseCore 0:
  10.3 56.4 all-gather.3
  97.1 55.0 reduce-scatter.3
  154.4 31.6 all-gather.5
  219.5 53.9 reduce-scatter.5
  275.7 31.6 all-gather.7
  339.5 39.4 reduce-scatter.7
where the time goes:
time: 396 us; the launch traced here: 390 us
  waiting for transfers between devices  264 us (67%)
  matrix products  56.7 us (14%)
  other arithmetic  36.8 us (9%)
  starting transfers between devices  14.9 us (4%)
  between operations  14.3 us (4%)
    reduce_scatter x2, waiting for transfers between devices, shards(): lax.psum_scatter(project(), 'tp', scatter_dimension=0, tiled=True)  109 us
    all_gather x2, waiting for transfers between devices, shards(): current = lax.all_gather(share_rows, 'tp', axis=0, tiled=True)  63 us
    all_gather x1, waiting for transfers between devices, sent_together(): result, at, done = (lax.all_gather(both, axis, axis=dim, tiled=True), 0, [])  46.3 us
    reduce_scatter x1, waiting for transfers between devices, shards(): lax.psum_scatter(project().astype(jnp.bfloat16), 'tp', scatter_dimension=...  39.6 us
    dot_general x3, matrix products, project(): lax.dot_general(attended, out_weight, (((1,), (1,)), ((), ())), preferred...  15.4 us
    reduce_sum x4, other arithmetic, norm_rows(): jnp.mean(wide_values * wide_values, axis=-1, keepdims=True) + EPS  10.9 us
    dot_general x3, matrix products, attend(): jnp.einsum('kgqs,skd->qkgd', weights, value_rows, preferred_element_type=...  10.6 us
    ppermute x3, starting transfers between devices, extended_2(): lax.ppermute(lax.slice_in_dim(block, block.shape[dim] - width, None, axis...  10.2 us
  transfers between devices with their start and end apart: 12, of which 9 were waited for; matrix products, arithmetic and copies ran while one was open for 5% of the time, Pallas kernels for 0%

commit v1 on v0

v1 whole, which is shorter than its diff:
```python
import functools

import jax
import jax.numpy as jnp
from jax import lax
from jax.experimental import pallas as pl
from jax.experimental.pallas import tpu as pltpu
from jax.sharding import PartitionSpec as P

D = 2048
HEAD_DIM = 64
WINDOW = 128
LAYERS = 3
EPS = 1e-06
BLK = 128
RING = 4
SEQ = 16384
MASKED = -1e30
MESH = pl.DeviceIdType.MESH
F32 = jnp.float32
BF16 = jnp.bfloat16

ROTATIONS = (("x", "y", "z"), ("y", "z", "x"), ("z", "x", "y"))
DIMS = ("x", "z", "y")
STAGES = ((0, 0, 3), (1, 0, 1), (1, 1, 3), (2, 0, 1), (2, 1, 2), (2, 2, 3))
N_IDS = len(STAGES) * 3 * 6


def mod4(v):
    return lax.rem(v + 2 * RING, RING)


def kernel(
    inputs, q_w, k_w, v_w, o_w, norm_gain, final_gain, sink_tile, q_cos, q_sin, kv_cos, kv_sin,
    out,
    g_q, g_kv, g_o, staged, normed, kv_rows, q_rows, att, part_own, part_send, part_recv, bias, sinks,
    send_sem, recv_sem, local_sem, halo_send, halo_recv, part_ssem, part_rsem, norm_ssem, norm_rsem,
    sink_ssem, sink_rsem,
):
    sp, tp = lax.axis_index("sp"), lax.axis_index("tp")
    z, y = sp // RING, lax.rem(sp, RING)
    x, c = tp // 2, lax.rem(tp, 2)
    at = {"x": x, "y": y, "z": z}
    chip = sp * RING + x

    def neighbour(dim, step):
        there = dict(at)
        there[dim] = mod4(at[dim] + step)
        return (there["z"] * RING + there["y"], there["x"] * 2 + c)

    def chip_at(step):
        other = lax.rem(chip + step + 64, 64)
        return (other // RING, lax.rem(other, RING) * 2 + c)

    peer = (sp, x * 2 + 1 - c)

    own_q = pltpu.make_async_copy(q_w, g_q.at[:, x, z, y], local_sem.at[0])
    own_o = pltpu.make_async_copy(o_w, g_o.at[:, x, z, y], local_sem.at[1])
    own_in = pltpu.make_async_copy(inputs.at[pl.ds(x * 2 * BLK, 2 * BLK)], staged, local_sem.at[2])
    own_q.start()
    own_o.start()
    own_in.start()

    barrier = pltpu.get_barrier_semaphore()
    greeted = [neighbour(d, s) for d in DIMS for s in (1, -1)] + [neighbour("x", 2), chip_at(1), chip_at(-1), peer]
    for device in greeted:
        pl.semaphore_signal(barrier, inc=1, device_id=device, device_id_type=MESH)

    for l in range(LAYERS):
        g_kv[l, x, z, y] = jnp.concatenate([k_w[l], v_w[l]], axis=1)
    own_q.wait()
    own_o.wait()
    pl.semaphore_wait(barrier, len(greeted))

    pending = []
    blocks = (g_q, g_kv, g_o)

    def view(stage, r, pos, half):
        phase, lo, hi = STAGES[stage]
        rotation = ROTATIONS[r]
        index = {d: at[d] for d in DIMS}
        index[rotation[phase]] = pos
        gathered = rotation[:phase]
        for d in gathered:
            index[d] = slice(None)
        rows = slice(None)
        if phase == 0:
            rows = slice(half * 64, half * 64 + 64)
        else:
            outer = [d for d in DIMS if d in gathered][0]
            index[outer] = slice(half * 2, half * 2 + 2)
        return blocks[r].at[(slice(lo, hi),) + tuple(index[d] for d in DIMS) + (rows,)]

    def copy_of(stage, r, pos, half, slot, device):
        k = (stage * 3 + r) * 6 + slot
        ref = view(stage, r, pos, half)
        return pltpu.make_async_remote_copy(
            src_ref=ref, dst_ref=ref, send_sem=send_sem.at[k], recv_sem=recv_sem.at[k],
            device_id=device, device_id_type=MESH,
        )

    def send(stage, r, back, half, slot, step):
        dim = ROTATIONS[r][STAGES[stage][0]]
        copy = copy_of(stage, r, mod4(at[dim] + back), half, slot, neighbour(dim, step))
        copy.start()
        pending.append(copy)

    def arrived(stage, r, back, half, slot):
        dim = ROTATIONS[r][STAGES[stage][0]]
        copy_of(stage, r, mod4(at[dim] + back), half, slot, peer).wait_recv()

    def first(stage):
        for r in range(3):
            send(stage, r, 0, 0, 0, 1)
            send(stage, r, 0, 1, 1, -1)

    def second(stage):
        for r in range(3):
            send(stage, r, 0, 1, 2, 1)
            send(stage, r, 0, 0, 3, -1)

    def forward(stage):
        for r in range(3):
            arrived(stage, r, -1, 0, 0)
            send(stage, r, -1, 0, 4, 1)
            arrived(stage, r, 1, 1, 1)
            send(stage, r, 1, 1, 5, -1)

    def finish(stage):
        for r in range(3):
            arrived(stage, r, -1, 1, 2)
            arrived(stage, r, 1, 0, 3)
            arrived(stage, r, 2, 0, 4)
            arrived(stage, r, 2, 1, 5)

    def sink_copy(i):
        return pltpu.make_async_remote_copy(
            src_ref=sink_tile, dst_ref=sinks.at[x], send_sem=sink_ssem.at[i - 1], recv_sem=sink_rsem.at[i - 1],
            device_id=neighbour("x", i), device_id_type=MESH,
        )

    def norm_into(src, first_row, rows, gain, write):
        def body(i, carry):
            at_row = pl.ds(pl.multiple_of(first_row + i * 16, 16), 16)
            v = src(i * 16, at_row)
            root = lax.rsqrt(jnp.mean(v * v, axis=-1, keepdims=True) + EPS)
            write(at_row, v * root * gain)
            return carry

        lax.fori_loop(0, rows // 16, body, 0)

    lane = lax.broadcasted_iota(jnp.int32, (2 * BLK, BLK), 1)
    low_half = lax.rem(lane, HEAD_DIM) < HEAD_DIM // 2
    low_head = lane < HEAD_DIM

    def turned(v, cos, sin):
        swapped = jnp.where(low_half, pltpu.roll(v, BLK - 32, 1), pltpu.roll(v, 32, 1))
        return v * cos[...] + swapped * sin[...]

    def project_kv(l):
        def body(i, carry):
            w = jnp.concatenate([g_kv[l, 2 * i + j].reshape(D, BLK) for j in range(2)], axis=1)
            raw = jnp.dot(normed[l], w, preferred_element_type=F32)
            for j in range(2):
                kv = turned(raw[:, j * BLK : (j + 1) * BLK], kv_cos, kv_sin)
                kv_rows[l, 2 * i + j, pl.ds(BLK, 2 * BLK)] = kv.astype(BF16)
            return carry

        lax.fori_loop(0, 2, body, 0)

    def project_q(l):
        def body(i, carry):
            w = jnp.concatenate([g_q[l, 2 * i + j].reshape(D, BLK) for j in range(2)], axis=1)
            raw = jnp.dot(normed[l], w, preferred_element_type=F32)
            for j in range(2):
                q = turned(raw[:, j * BLK : (j + 1) * BLK], q_cos, q_sin)
                head0 = jnp.where(low_head, q, 0.0).astype(BF16)
                head1 = jnp.where(low_head, pltpu.roll(q, HEAD_DIM, 1), 0.0).astype(BF16)
                for b in range(2):
                    q_rows[2 * i + j, b, pl.ds(0, BLK)] = head0[b * BLK : (b + 1) * BLK]
                    q_rows[2 * i + j, b, pl.ds(BLK, BLK)] = head1[b * BLK : (b + 1) * BLK]
            return carry

        lax.fori_loop(0, 2, body, 0)

    def halo(l):
        to_right = pltpu.make_async_remote_copy(
            src_ref=kv_rows.at[l, :, pl.ds(2 * BLK, BLK)], dst_ref=kv_rows.at[l, :, pl.ds(0, BLK)],
            send_sem=halo_send.at[l, 0], recv_sem=halo_recv.at[l, 0], device_id=chip_at(1), device_id_type=MESH,
        )
        to_left = pltpu.make_async_remote_copy(
            src_ref=kv_rows.at[l, :, pl.ds(BLK, BLK)], dst_ref=kv_rows.at[l, :, pl.ds(3 * BLK, BLK)],
            send_sem=halo_send.at[l, 1], recv_sem=halo_recv.at[l, 1], device_id=chip_at(-1), device_id_type=MESH,
        )
        return to_right, to_left

    low_lane = lax.broadcasted_iota(jnp.int32, (BLK, BLK), 1) < HEAD_DIM

    def attention(l, lo, hi):
        def body(i, carry):
            h, b = i // 2, lax.rem(i, 2)
            kv = kv_rows[l, h, pl.ds(pl.multiple_of(b * BLK, BLK), 3 * BLK)]
            s = lax.dot_general(q_rows[h, b], kv, (((1,), (1,)), ((), ())), preferred_element_type=F32)
            limits = bias[b]
            tops = []
            for g in range(2):
                own = s[g * BLK : (g + 1) * BLK] + limits
                sink = sinks[h, pl.ds(2 * l + g, 1), pl.ds(0, 1)]
                m = jnp.maximum(jnp.max(own, axis=1, keepdims=True), sink)
                p = jnp.exp(own - m)
                total = jnp.sum(p, axis=1, keepdims=True) + jnp.exp(sink - m)
                o = jnp.dot(p.astype(BF16), kv, preferred_element_type=F32)
                tops.append(o / total)
            both = jnp.where(low_lane, pltpu.roll(tops[0], HEAD_DIM, 1), tops[1])
            att[h, pl.ds(pl.multiple_of(b * BLK, BLK), BLK)] = both.astype(BF16)
            return carry

        lax.fori_loop(2 * lo, 2 * hi, body, 0)

    def project_out(l, block, dst):
        rows = pl.ds(pl.multiple_of(block * BLK, BLK), BLK)
        lhs = jnp.concatenate([att[h, rows] for h in range(RING)], axis=1)

        def body(i, carry):
            zz, yy = i // 2, lax.rem(i, 2) * 2
            w = jnp.concatenate([g_o[l, h, zz, pl.ds(yy, 2)].reshape(2 * BLK, BLK) for h in range(RING)], axis=1)
            r = lax.dot_general(lhs, w, (((1,), (1,)), ((), ())), preferred_element_type=F32)
            dst[:, pl.ds(pl.multiple_of(i * 2 * BLK, 2 * BLK), 2 * BLK)] = r
            return carry

        lax.fori_loop(0, 8, body, 0)

    def part_copy(l):
        return pltpu.make_async_remote_copy(
            src_ref=part_send.at[l], dst_ref=part_recv.at[l], send_sem=part_ssem.at[l], recv_sem=part_rsem.at[l],
            device_id=peer, device_id_type=MESH,
        )

    def norm_copy(l, block):
        rows = normed.at[l, pl.ds(pl.multiple_of(block * BLK, BLK), BLK)]
        return pltpu.make_async_remote_copy(
            src_ref=rows, dst_ref=rows, send_sem=norm_ssem.at[l], recv_sem=norm_rsem.at[l],
            device_id=peer, device_id_type=MESH,
        )

    def summed(l):
        def src(i, at_row):
            rows = pl.ds(pl.multiple_of(i, 16), 16)
            return (part_own[rows] + part_recv[l, rows]).astype(BF16).astype(F32)

        return src

    def layer(l, between_q, between_att, between_out, last):
        project_kv(l)
        copies = halo(l)
        for copy in copies:
            copy.start()
            pending.append(copy)
        project_q(l)
        between_q()
        for copy in copies:
            copy.wait_recv()
        attention(l, 0, 4)
        between_att()
        project_out(l, 1 - c, part_send.at[l])
        copy = part_copy(l)
        copy.start()
        pending.append(copy)
        project_out(l, c, part_own)
        between_out()
        copy.wait_recv()
        if last:
            gain = final_gain[...]

            def write(at_row, v):
                out[at_row] = v

            norm_into(summed(l), 0, BLK, gain, write)
            return
        gain = norm_gain[pl.ds(l + 1, 1)]

        def write(at_row, v):
            normed[l + 1, at_row] = v.astype(BF16)

        norm_into(summed(l), c * BLK, BLK, gain, write)
        copy = norm_copy(l + 1, c)
        copy.start()
        pending.append(copy)
        norm_copy(l + 1, 1 - c).wait_recv()

    first(0)
    second(0)
    for i in range(1, RING):
        copy = sink_copy(i)
        copy.start()
        pending.append(copy)
    sinks[x] = sink_tile[...]
    own_in.wait()

    def write_first(at_row, v):
        normed[0, at_row] = v.astype(BF16)

    norm_into(lambda i, at_row: staged[at_row].astype(F32), 0, BLK, norm_gain[pl.ds(0, 1)], write_first)
    forward(0)
    norm_into(lambda i, at_row: staged[at_row].astype(F32), BLK, BLK, norm_gain[pl.ds(0, 1)], write_first)
    finish(0)
    first(1)
    second(1)
    row_i = lax.broadcasted_iota(jnp.int32, (BLK, 3 * BLK), 0)
    col_j = lax.broadcasted_iota(jnp.int32, (BLK, 3 * BLK), 1)
    for b in range(2):
        position = (chip * 2 + b - 1) * BLK + col_j
        gap = col_j - row_i
        allowed = (gap >= 0) & (gap <= 2 * WINDOW) & (position >= 0) & (position < SEQ)
        bias[b] = jnp.where(allowed, 0.0, MASKED)
    forward(1)
    first(2)
    finish(1)
    first(3)
    second(2)
    second(3)
    forward(2)
    forward(3)
    for i in range(1, RING):
        pltpu.make_async_remote_copy(
            src_ref=sink_tile, dst_ref=sinks.at[mod4(x - i)], send_sem=sink_ssem.at[i - 1],
            recv_sem=sink_rsem.at[i - 1], device_id=peer, device_id_type=MESH,
        ).wait_recv()
    finish(2)
    first(4)
    finish(3)
    layer(0, lambda: second(4), lambda: forward(4), lambda: first(5), False)
    finish(4)
    layer(1, lambda: second(5), lambda: forward(5), lambda: None, False)
    finish(5)
    layer(2, lambda: None, lambda: None, lambda: None, True)
    for copy in pending:
        copy.wait_send()


def shards(inputs, norm_gain, query_weight, key_weight, value_weight, output_weight, sink_logit, final_gain):
    sp, tp = lax.axis_index("sp"), lax.axis_index("tp")
    chip = sp * RING + tp // 2
    half = HEAD_DIM // 2
    inverse = 10000.0 ** (-jnp.arange(half).astype(F32) / half)
    places = (chip * 2 * BLK + jnp.arange(2 * BLK, dtype=jnp.int32)).astype(F32)
    angles = places[:, None] * inverse[None, :]
    scale = float(D) ** (-0.5)
    cos, sin = jnp.cos(angles) * scale, jnp.sin(angles) * scale
    cos_head = jnp.concatenate([cos, cos], axis=1)
    sin_head = jnp.concatenate([-sin, sin], axis=1)
    one = jnp.ones_like(cos_head)
    q_cos = jnp.concatenate([cos_head, cos_head], axis=1) * 0.125
    q_sin = jnp.concatenate([sin_head, sin_head], axis=1) * 0.125
    kv_cos = jnp.concatenate([cos_head, one], axis=1)
    kv_sin = jnp.concatenate([sin_head, 0.0 * one], axis=1)
    sink_tile = jnp.pad(jnp.broadcast_to(sink_logit.reshape(2 * LAYERS, 1), (2 * LAYERS, BLK)), ((0, 2), (0, 0)))
    vmem = pl.BlockSpec(memory_space=pltpu.VMEM)
    anywhere = pl.BlockSpec(memory_space=pl.ANY)
    weights = pltpu.VMEM((LAYERS, RING, RING, RING, BLK, BLK), BF16)
    dma = pltpu.SemaphoreType.DMA
    return pl.pallas_call(
        kernel,
        out_shape=jax.ShapeDtypeStruct((BLK, D), F32),
        in_specs=[anywhere, anywhere, vmem, vmem, anywhere] + [vmem] * 7,
        out_specs=vmem,
        scratch_shapes=[
            weights, weights, weights,
            pltpu.VMEM((2 * BLK, D), BF16),
            pltpu.VMEM((LAYERS, 2 * BLK, D), BF16),
            pltpu.VMEM((LAYERS, RING, 4 * BLK, BLK), BF16),
            pltpu.VMEM((RING, 2, 2 * BLK, BLK), BF16),
            pltpu.VMEM((RING, 2 * BLK, BLK), BF16),
            pltpu.VMEM((BLK, D), F32),
            pltpu.VMEM((LAYERS, BLK, D), F32),
            pltpu.VMEM((LAYERS, BLK, D), F32),
            pltpu.VMEM((2, BLK, 3 * BLK), F32),
            pltpu.VMEM((RING, 8, BLK), F32),
            dma((N_IDS,)), dma((N_IDS,)), dma((3,)),
            dma((LAYERS, 2)), dma((LAYERS, 2)),
            dma((LAYERS,)), dma((LAYERS,)), dma((LAYERS,)), dma((LAYERS,)),
            dma((RING - 1,)), dma((RING - 1,)),
        ],
        compiler_params=pltpu.CompilerParams(
            collective_id=0, has_side_effects=True, vmem_limit_bytes=60 * 1024 * 1024
        ),
    )(
        inputs, query_weight, key_weight, value_weight, output_weight, norm_gain, final_gain.reshape(1, D),
        sink_tile, q_cos, q_sin, kv_cos, kv_sin,
    )


def solution(mesh):
    in_specs = (
        P("sp", None),
        P(),
        P(None, "sp", "tp"),
        P(None, "sp", "tp"),
        P(None, "sp", "tp"),
        P(None, "sp", "tp"),
        P(None, "tp"),
        P(),
    )
    out_specs = P(("sp", "tp"), None)
    return jax.shard_map(shards, mesh=mesh, in_specs=in_specs, out_specs=out_specs, check_vma=False)
```

time: 396 us -> 128 us (0.32); the launches traced: 390 us -> 126 us
  waiting for transfers between devices: 264 us -> 0 us
  Pallas kernels: 0 us -> 117 us
  matrix products: 56.7 us -> 0 us
  other arithmetic: 36.8 us -> 1.59 us
  starting transfers between devices: 14.9 us -> 0 us
  between operations: 14.3 us -> 0.02 us
    reduce_scatter x3 -> x0, waiting for transfers between devices: 149 us -> none  [the longest x2 109 us: shards(): lax.psum_scatter(project(), 'tp', scatter_dimension=0, tiled=True)]
    pallas_call x0 -> x1, Pallas kernels: none -> 117 us  [shards(): pl.pallas_call(kernel, out_shape=jax.ShapeDtypeStruct((BLK, D), F32), in_...]
    all_gather x3 -> x0, waiting for transfers between devices: 109 us -> none  [the longest x2 63 us: shards(): current = lax.all_gather(share_rows, 'tp', axis=0, tiled=True)]
    dot_general x18 -> x0, matrix products: 56.7 us -> none  [the longest x3 15.4 us: project(): lax.dot_general(attended, out_weight, (((1,), (1,)), ((), ())), preferred...]
    reduce_sum x7 -> x0, other arithmetic: 18.4 us -> none  [the longest x4 10.9 us: norm_rows(): jnp.mean(wide_values * wide_values, axis=-1, keepdims=True) + EPS]
    ppermute x6 -> x0, starting transfers between devices: 14.2 us -> none  [the longest x3 10.2 us: extended_2(): lax.ppermute(lax.slice_in_dim(block, block.shape[dim] - width, None, axis...]
    convert_element_type x6 -> x1, other arithmetic: 9.17 us -> 0.01 us  [shards(): places = (chip * 2 * BLK + jnp.arange(2 * BLK, dtype=jnp.int32)).astype(F32)]
    ppermute x6 -> x0, waiting for transfers between devices: 5.36 us -> none  [the longest x3 5.36 us: extended_2(): lax.ppermute(lax.slice_in_dim(block, 0, width, axis=dim), axis, backward)]
  transfers between devices with their start and end apart: 12 -> 0, of which waited for: 9 -> 0; matrix products, arithmetic and copies ran while one was open for 5% -> 0% of each run, Pallas kernels for 0% -> 0%
where the time goes in v1:
time: 128 us; the launch traced here: 126 us
  Pallas kernels  117 us (91%)
  local copies, waits for them, and re-layouts  7.04 us (6%)
  other arithmetic  1.59 us (1%)
    pallas_call x1, Pallas kernels, shards(): pl.pallas_call(kernel, out_shape=jax.ShapeDtypeStruct((BLK, D), F32), in_...  117 us
    unnamed x4, local copies, waits for them, and re-layouts  6.13 us

profile of v1, /device:TPU:0, one launch (start us, length us, event | category | flops | bytes accessed | tf_op | source)
XLA Modules:
  0.0 125.9 jit_solution(10640612621593590739)
XLA Ops:
  0.0 0.1 pad.10.clone
  0.1 0.1 pad.13.clone
  0.2 0.8 copy.12
  0.9 0.1 broadcast_in_dim.4
  1.0 0.7 pad.7.sink_tile
  1.7 1.5 %copy.13.k_w = bf16[3,128,64]{2,1,0:T(8,128)(2,1)} copy(bf16[3,128,64]{1,2,0:T(8,128)(2,1)} %param.11) | data formatting | bytes 98304 | tf_op args[3]
  3.2 1.5 %copy.14.v_w = bf16[3,128,64]{2,1,0:T(8,128)(2,1)} copy(bf16[3,128,64]{1,2,0:T(8,128)(2,1)} %param.12) | data formatting | bytes 98304 | tf_op args[4]
  4.8 0.5 fusion.4
  5.3 1.0 fusion.2
  6.4 117.3 %shard_map.82 = f32[128,2048]{1,0:T(8,128)} custom-call(bf16[1024,2048]{1,0:T(8,128)(2,1)} %inputs.1, bf16[3,128,128]{2,1,0:T(8,128)(2,1)} %q_w.1, bf16[3,128,64]{2,1,0:T(8,128)(2,1)} %copy.13.k_w, bf16[3,128,64]{2,1,0:T(8,128)(2,1)} %copy.14.v_w, bf16[3,128,128]{2,1,0:T(8,128)(2,1)} %o_w.1, f32[3,2048]{1,0:T(4,128)} %norm_gain.1, f32[1,2048]{1,0:T(1,128)} %bitcast.1, ...), custom_call_target="tpu_custom_call" | custom-call | tf_op jit(solution)/shard_map/pallas_call | solution.py:362
  123.6 2.3 %copy.16 = f32[128,2048]{1,0:T(8,128)} copy(f32[128,2048]{1,0:T(8,128)} %shard_map.82) | data formatting | bytes 2097152
  (5 shorter events, 0.0 us)

commit v2 on v0

v2 whole, which is shorter than its diff:
```python
import math

import jax
import jax.numpy as jnp
from jax import lax
from jax.experimental import pallas as pl
from jax.experimental.pallas import tpu as pltpu
from jax.sharding import PartitionSpec as P

D = 2048
HEAD_DIM = 64
WINDOW = 128
LAYERS = 3
EPS = 1e-06
BLK = 128
RING = 4
SEQ = 16384
MASKED = -1e30
MESH = pl.DeviceIdType.MESH
F32 = jnp.float32
BF16 = jnp.bfloat16

ROTATIONS = (("x", "y", "z"), ("y", "z", "x"), ("z", "x", "y"))
DIMS = ("x", "z", "y")
KV, Q, O = 0, 1, 2
ROWS = (((0, 48), (48, 80), (80, 128)), ((0, 48), (48, 80), (80, 128)), ((0, 40), (40, 88), (88, 128)))
SPREADS = tuple((kind, lo, hi) for lo, hi in ((0, 1), (1, 3)) for kind in (KV, Q, O))
GROUPS = tuple((kind, layer) for layer in range(LAYERS) for kind in (KV, Q, O))
CHUNKS = 4
LOG2E = 1.4426950408889634


def mod4(v):
    return lax.rem(v + 2 * RING, RING)


def kernel(
    inputs, q_w, k_w, v_w, o_w, norm_gain_in, sink_in,
    out,
    norm_gain, sink_logit, w_all, staged, normed, kv_rows, q_rows, att, part_own, part_send, part_recv, bias, sinks,
    sink_tile, tables,
    spread_send, spread_recv, ring_send, ring_recv, local_sem, halo_send, halo_recv, part_ssem, part_rsem, sink_sem,
):
    sp, tp = lax.axis_index("sp"), lax.axis_index("tp")
    z, y = sp // RING, lax.rem(sp, RING)
    x, c = tp // 2, lax.rem(tp, 2)
    at = {"x": x, "y": y, "z": z}
    chip = sp * RING + x

    def neighbour(dim, step):
        there = dict(at)
        there[dim] = mod4(at[dim] + step)
        return (there["z"] * RING + there["y"], there["x"] * 2 + c)

    def chip_at(step):
        other = lax.rem(chip + step + 64, 64)
        return (other // RING, lax.rem(other, RING) * 2 + c)

    peer = (sp, x * 2 + 1 - c)

    def own_block(first, count):
        return w_all.at[:, x, z, y, pl.ds(first, count)]

    own = [
        pltpu.make_async_copy(k_w, own_block(0, HEAD_DIM), local_sem.at[0]),
        pltpu.make_async_copy(v_w, own_block(HEAD_DIM, HEAD_DIM), local_sem.at[1]),
        pltpu.make_async_copy(q_w, own_block(Q * BLK, BLK), local_sem.at[2]),
        pltpu.make_async_copy(o_w, own_block(O * BLK, BLK), local_sem.at[3]),
    ]
    small = [
        pltpu.make_async_copy(sink_in, sink_logit, local_sem.at[4]),
        pltpu.make_async_copy(norm_gain_in, norm_gain, local_sem.at[5]),
        pltpu.make_async_copy(inputs.at[pl.ds(x * 2 * BLK, 2 * BLK)], staged, local_sem.at[6]),
    ]
    for copy in own + small:
        copy.start()

    barrier = pltpu.get_barrier_semaphore()
    greeted = [neighbour(d, s) for d in DIMS for s in (1, 2, 3)] + [peer]
    for device in greeted:
        pl.semaphore_signal(barrier, inc=1, device_id=device, device_id_type=MESH)
    for copy in own:
        copy.wait()
    pl.semaphore_wait(barrier, len(greeted))

    unsent = []

    def remote(src, dst, ssem, rsem, device):
        return pltpu.make_async_remote_copy(
            src_ref=src, dst_ref=dst, send_sem=ssem, recv_sem=rsem, device_id=device, device_id_type=MESH
        )

    def all_in(ref, sem):
        remote(ref, ref, sem, sem, peer).wait_recv()

    def all_out(ref, sem):
        unsent.append(remote(ref, ref, sem, sem, peer))

    def some_blocks(kind, lo, hi, xs, zs, ys):
        return w_all.at[lo:hi, 0:xs, 0:zs, 0:ys, pl.ds(kind * BLK, BLK)]

    def view(kind, lo, hi, r, phase, pos, half):
        rotation = ROTATIONS[r]
        index = {d: at[d] for d in DIMS}
        index[rotation[phase]] = pos
        for d in rotation[:phase]:
            index[d] = slice(None)
        if half is not None:
            outer = [d for d in DIMS if d in rotation[:phase]][0]
            index[outer] = slice(half * 2, half * 2 + 2)
        first, last = ROWS[kind][r]
        rows = slice(kind * BLK + first, kind * BLK + last)
        return w_all.at[(slice(lo, hi),) + tuple(index[d] for d in DIMS) + (rows,)]

    def spread(i):
        kind, lo, hi = SPREADS[i]
        for r in range(3):
            dim = ROTATIONS[r][0]
            ref = view(kind, lo, hi, r, 0, at[dim], None)
            for step in (1, 3, 2):
                remote(ref, ref, spread_send.at[i], spread_recv.at[i], neighbour(dim, step)).start()
        all_out(some_blocks(kind, lo, hi, 3, 1, 1), spread_send.at[i])

    def spread_in(i):
        kind, lo, hi = SPREADS[i]
        all_in(some_blocks(kind, lo, hi, 3, 1, 1), spread_recv.at[i])

    def hop(group, phase, back, half, slot, step):
        kind, layer = GROUPS[group]
        for r in range(3):
            dim = ROTATIONS[r][phase]
            ref = view(kind, layer, layer + 1, r, phase, mod4(at[dim] + back), half)
            ssem, rsem = ring_send.at[2 * group + phase - 1], ring_recv.at[4 * group + slot]
            remote(ref, ref, ssem, rsem, neighbour(dim, step)).start()

    def landed(group, slot, xs, zs, ys):
        kind, layer = GROUPS[group]
        all_in(some_blocks(kind, layer, layer + 1, xs, zs, ys), ring_recv.at[4 * group + slot])

    def plane(g):
        hop(g, 1, 0, None, 0, 1)
        hop(g, 1, 0, None, 0, -1)

    def plane_on(g):
        landed(g, 0, 2, 1, 4)
        hop(g, 1, -1, 0, 1, 1)
        hop(g, 1, 1, 1, 1, -1)
        kind, layer = GROUPS[g]
        all_out(some_blocks(kind, layer, layer + 1, 3, 1, 4), ring_send.at[2 * g])

    def plane_in(g):
        landed(g, 1, 1, 1, 4)

    def cube(g):
        hop(g, 2, 0, 0, 2, 1)
        hop(g, 2, 0, 1, 2, -1)
        hop(g, 2, 0, 1, 3, 1)
        hop(g, 2, 0, 0, 3, -1)

    def cube_on(g):
        landed(g, 2, 1, 4, 4)
        hop(g, 2, -1, 0, 3, 1)
        hop(g, 2, 1, 1, 3, -1)
        kind, layer = GROUPS[g]
        all_out(some_blocks(kind, layer, layer + 1, 3, 4, 4), ring_send.at[2 * g + 1])

    def cube_in(g):
        landed(g, 3, 2, 4, 4)

    def norm_rows(src, rows, write):
        def body(i, carry):
            at_row = pl.ds(pl.multiple_of(i * 16, 16), 16)
            v = src(at_row)
            root = lax.rsqrt(jnp.mean(v * v, axis=-1, keepdims=True) + EPS)
            write(at_row, v * root)
            return carry

        lax.fori_loop(0, rows // 16, body, 0)

    lane = lax.broadcasted_iota(jnp.int32, (2 * BLK, BLK), 1)
    low_half = lax.rem(lane, HEAD_DIM) < HEAD_DIM // 2
    low_head = lane < HEAD_DIM

    def make_tables():
        row = lax.broadcasted_iota(jnp.int32, (2 * BLK, BLK), 0) + chip * 2 * BLK
        place = lax.rem(lane, HEAD_DIM // 2).astype(F32)
        angle = row.astype(F32) * jnp.exp(place * (-math.log(10000.0) * 2 / HEAD_DIM))
        scale = float(D) ** (-0.5)
        cos = jnp.cos(angle) * scale
        sin = jnp.where(low_half, -scale, scale) * jnp.sin(angle)
        tables[0] = cos * (0.125 * LOG2E)
        tables[1] = sin * (0.125 * LOG2E)
        tables[2] = jnp.where(low_head, cos, 1.0)
        tables[3] = jnp.where(low_head, sin, 0.0)

    def make_bias():
        row_i = lax.broadcasted_iota(jnp.int32, (BLK, 3 * BLK), 0)
        col_j = lax.broadcasted_iota(jnp.int32, (BLK, 3 * BLK), 1)
        gap = col_j - row_i
        for b in range(2):
            position = (chip * 2 + b - 1) * BLK + col_j
            allowed = (gap >= 0) & (gap <= 2 * WINDOW) & (position >= 0) & (position < SEQ)
            bias[b] = jnp.where(allowed, 0.0, MASKED)

    def turned(v, which):
        swapped = jnp.where(low_half, pltpu.roll(v, BLK - 32, 1), pltpu.roll(v, 32, 1))
        return v * tables[which] + swapped * tables[which + 1]

    def project_kv(l):
        def body(i, carry):
            w = jnp.concatenate(
                [
                    jnp.concatenate([w_all[l, 2 * i + j, n // RING, n % RING, pl.ds(0, BLK)] for n in range(16)], axis=1)
                    for j in range(2)
                ],
                axis=0,
            )
            raw = lax.dot_general(normed[l], w, (((1,), (1,)), ((), ())), preferred_element_type=F32)
            for j in range(2):
                kv = turned(raw[:, j * BLK : (j + 1) * BLK], 2)
                kv_rows[l, 2 * i + j, pl.ds(BLK, 2 * BLK)] = kv.astype(BF16)
            return carry

        lax.fori_loop(0, 2, body, 0)

    def project_q(l):
        def body(i, carry):
            w = jnp.concatenate(
                [w_all[l, 2 * i + j, :, :, pl.ds(Q * BLK, BLK)].reshape(D, BLK) for j in range(2)], axis=1
            )
            raw = jnp.dot(normed[l], w, preferred_element_type=F32)
            for j in range(2):
                q = turned(raw[:, j * BLK : (j + 1) * BLK], 0)
                head0 = jnp.where(low_head, q, 0.0).astype(BF16)
                head1 = jnp.where(low_head, pltpu.roll(q, HEAD_DIM, 1), 0.0).astype(BF16)
                for b in range(2):
                    q_rows[2 * i + j, b, pl.ds(0, BLK)] = head0[b * BLK : (b + 1) * BLK]
                    q_rows[2 * i + j, b, pl.ds(BLK, BLK)] = head1[b * BLK : (b + 1) * BLK]
            return carry

        lax.fori_loop(0, 2, body, 0)

    def halo(l):
        rows = kv_rows.at[l]
        low, high = pl.ds(BLK, BLK), pl.ds(2 * BLK, BLK)
        sems = halo_send.at[l], halo_recv.at[l]
        remote(rows.at[:, high], rows.at[:, pl.ds(0, BLK)], *sems, chip_at(1)).start()
        remote(rows.at[:, low], rows.at[:, pl.ds(3 * BLK, BLK)], *sems, chip_at(-1)).start()
        all_out(rows.at[:, pl.ds(0, 2 * BLK)], sems[0])

    def halo_in(l):
        all_in(kv_rows.at[l, :, pl.ds(0, 2 * BLK)], halo_recv.at[l])

    low_lane = lax.broadcasted_iota(jnp.int32, (BLK, BLK), 1) < HEAD_DIM
    low_key = lax.broadcasted_iota(jnp.int32, (3 * BLK, BLK), 1) < HEAD_DIM

    def attention(l, lo, hi):
        def body(h, carry):
            for b in range(2):
                kv = kv_rows[l, h, pl.ds(b * BLK, 3 * BLK)]
                ones_v = jnp.where(low_key, jnp.ones_like(kv), kv)
                s = lax.dot_general(q_rows[h, b], kv, (((1,), (1,)), ((), ())), preferred_element_type=F32)
                sums, extra = [], []
                for g in range(2):
                    mine = s[g * BLK : (g + 1) * BLK] + bias[b]
                    sink = sinks[h, pl.ds(2 * l + g, 1), pl.ds(0, 1)]
                    m = jnp.maximum(jnp.max(mine, axis=1, keepdims=True), sink)
                    p = jnp.exp2(mine - m).astype(BF16)
                    sums.append(jnp.dot(p, ones_v, preferred_element_type=F32))
                    extra.append(jnp.exp2(sink - m))
                top = jnp.where(low_lane, pltpu.roll(sums[0], HEAD_DIM, 1), sums[1])
                below = jnp.where(low_lane, sums[0], pltpu.roll(sums[1], HEAD_DIM, 1))
                below = below + jnp.where(low_lane, extra[0], extra[1])
                att[h, pl.ds(b * BLK, BLK)] = (top / below).astype(BF16)
            return carry

        lax.fori_loop(lo, hi, body, 0)

    def part_rows(l, block):
        return pl.ds(pl.multiple_of(block * BLK, BLK), BLK) if l == LAYERS - 1 else slice(None)

    def send_part(l, j):
        cols = pl.ds(j * (D // CHUNKS), D // CHUNKS)
        rows = part_rows(l, 1 - c)
        remote(
            part_send.at[l, rows, cols], part_recv.at[l, rows, cols], part_ssem.at[l], part_rsem.at[l], peer
        ).start()

    def project_out(l):
        lhs = jnp.concatenate([att[h] for h in range(RING)], axis=1)
        for j in range(CHUNKS):

            def body(i, carry):
                pair = pl.ds(lax.rem(i, 2) * 2, 2)
                w = jnp.concatenate(
                    [w_all[l, h, i // 2, pair, pl.ds(O * BLK, BLK)].reshape(2 * BLK, BLK) for h in range(RING)],
                    axis=1,
                )
                r = lax.dot_general(lhs, w, (((1,), (1,)), ((), ())), preferred_element_type=F32)
                cols = pl.ds(pl.multiple_of(i * 2 * BLK, 2 * BLK), 2 * BLK)
                part_own[:, cols] = r
                part_send[l, :, cols] = r.astype(BF16)
                return carry

            lax.fori_loop(2 * j, 2 * j + 2, body, 0)
            if j > 0:
                send_part(l, j - 1)

    def parts_in(l):
        all_in(part_recv.at[l, part_rows(l, c)], part_rsem.at[l])

    def layer(l, steps):
        project_kv(l)
        steps[0]()
        halo(l)
        steps[1]()
        project_q(l)
        halo_in(l)
        steps[2]()
        attention(l, 0, 2)
        steps[3]()
        attention(l, 2, 4)
        steps[4]()
        project_out(l)
        steps[5]()
        send_part(l, CHUNKS - 1)
        all_out(part_send.at[l, part_rows(l, 1 - c)], part_ssem.at[l])
        parts_in(l)
        if l == LAYERS - 1:
            mine = part_rows(l, c)
            out[...] = (part_own[mine] + part_recv[l, mine].astype(F32)).astype(BF16)
            return

        def state(at_row):
            return (part_own[at_row] + part_recv[l, at_row].astype(F32)).astype(BF16).astype(F32)

        gain = norm_gain[pl.ds(l + 1, 1)]

        def write_normed(at_row, v):
            normed[l + 1, at_row] = (v * gain).astype(BF16)

        norm_rows(state, 2 * BLK, write_normed)
        steps[6]()

    def visits(*steps):
        return [lambda calls=calls: [f(*a) for f, *a in calls] for calls in steps]

    for i in range(3):
        spread(i)
    for copy in small:
        copy.wait()
    for l in range(LAYERS):
        for g in range(2):
            sink_tile[pl.ds(2 * l + g, 1)] = jnp.broadcast_to(sink_logit[pl.ds(g, 1), pl.ds(l, 1)], (1, BLK)) * LOG2E
    sinks[x] = sink_tile[...]
    for g in range(3):
        spread_in(g)
        plane(g)
    for i in range(3, 6):
        spread(i)
    for i in range(1, RING):
        remote(sink_tile, sinks.at[x], sink_sem.at[0], sink_sem.at[1], neighbour("x", i)).start()
    all_out(sinks.at[0:3], sink_sem.at[0])
    gain = norm_gain[pl.ds(0, 1)]

    def write_first(at_row, v):
        normed[0, at_row] = (v * gain).astype(BF16)

    plane_on(0)
    plane_on(1)
    plane_in(0)
    cube(0)
    norm_rows(lambda at_row: staged[at_row].astype(F32), 2 * BLK, write_first)
    plane_on(2)
    spread_in(3)
    plane(3)
    plane_in(1)
    cube(1)
    make_bias()
    cube_on(0)
    spread_in(4)
    plane(4)
    plane_on(3)
    plane_in(2)
    cube(2)
    make_tables()
    spread_in(5)
    plane(5)
    plane_on(4)
    all_in(sinks.at[0:3], sink_sem.at[1])
    cube_in(0)
    last = len(GROUPS) - 1
    for l in range(LAYERS):
        g = 3 * l
        plan = (
            [],
            [(cube_on, 1), (plane_in, 3), (cube, 3), (cube_on, 2), (plane_on, 5), (plane, 6), (cube_in, 1)],
            [(plane_on, 6), (plane, 7), (plane_in, 4), (cube, 4)],
            [(cube_on, 3)],
            [(cube_in, 2)],
            [(plane_on, 7), (plane, 8), (plane_in, 5), (cube, 5)],
            [(cube_in, 3)],
        )
        layer(l, visits(*([(f, g + n) for f, n in step if g + n <= last] for step in plan)))
    for copy in unsent:
        copy.wait_send()


def last_norm(rows, gain, out):
    v = rows[...].astype(F32)
    out[...] = v * lax.rsqrt(jnp.mean(v * v, axis=-1, keepdims=True) + EPS) * gain[...]


def shards(inputs, norm_gain, query_weight, key_weight, value_weight, output_weight, sink_logit, final_gain):
    vmem = pl.BlockSpec(memory_space=pltpu.VMEM)
    hbm = pl.BlockSpec(memory_space=pltpu.HBM)
    dma = pltpu.SemaphoreType.DMA
    rows = pl.pallas_call(
        kernel,
        out_shape=jax.ShapeDtypeStruct((BLK, D), BF16),
        in_specs=[hbm] * 7,
        out_specs=vmem,
        scratch_shapes=[
            pltpu.VMEM((LAYERS, D), F32),
            pltpu.VMEM((2, LAYERS), F32),
            pltpu.VMEM((LAYERS, RING, RING, RING, 3 * BLK, BLK), BF16),
            pltpu.VMEM((2 * BLK, D), BF16),
            pltpu.VMEM((LAYERS, 2 * BLK, D), BF16),
            pltpu.VMEM((LAYERS, RING, 4 * BLK, BLK), BF16),
            pltpu.VMEM((RING, 2, 2 * BLK, BLK), BF16),
            pltpu.VMEM((RING, 2 * BLK, BLK), BF16),
            pltpu.VMEM((2 * BLK, D), F32),
            pltpu.VMEM((LAYERS, 2 * BLK, D), BF16),
            pltpu.VMEM((LAYERS, 2 * BLK, D), BF16),
            pltpu.VMEM((2, BLK, 3 * BLK), F32),
            pltpu.VMEM((RING, 8, BLK), F32),
            pltpu.VMEM((8, BLK), F32),
            pltpu.VMEM((4, 2 * BLK, BLK), F32),
            dma((len(SPREADS),)), dma((len(SPREADS),)), dma((2 * len(GROUPS),)), dma((4 * len(GROUPS),)),
            dma((7,)), dma((LAYERS,)), dma((LAYERS,)), dma((LAYERS,)), dma((LAYERS,)), dma((2,)),
        ],
        compiler_params=pltpu.CompilerParams(
            collective_id=0, has_side_effects=True, vmem_limit_bytes=67043328
        ),
    )(
        inputs, query_weight, jnp.swapaxes(key_weight, 1, 2), jnp.swapaxes(value_weight, 1, 2), output_weight,
        norm_gain, jnp.swapaxes(sink_logit, 0, 1),
    )
    step = BLK // 4
    return pl.pallas_call(
        last_norm,
        grid=(4,),
        out_shape=jax.ShapeDtypeStruct((BLK, D), F32),
        in_specs=[pl.BlockSpec((step, D), lambda i: (i, 0)), pl.BlockSpec((1, D), lambda i: (0, 0))],
        out_specs=pl.BlockSpec((step, D), lambda i: (i, 0)),
    )(rows, final_gain.reshape(1, D))


def solution(mesh):
    in_specs = (
        P("sp", None),
        P(),
        P(None, "sp", "tp"),
        P(None, "sp", "tp"),
        P(None, "sp", "tp"),
        P(None, "sp", "tp"),
        P(None, "tp"),
        P(),
    )
    out_specs = P(("sp", "tp"), None)
    return jax.shard_map(shards, mesh=mesh, in_specs=in_specs, out_specs=out_specs, check_vma=False)
```

time: 396 us -> 108 us (0.27); the launches traced: 390 us -> 106 us
  waiting for transfers between devices: 264 us -> 0 us
  Pallas kernels: 0 us -> 106 us
  matrix products: 56.7 us -> 0 us
  other arithmetic: 36.8 us -> 0 us
  starting transfers between devices: 14.9 us -> 0 us
  between operations: 14.3 us -> 0.01 us
    reduce_scatter x3 -> x0, waiting for transfers between devices: 149 us -> none  [the longest x2 109 us: shards(): lax.psum_scatter(project(), 'tp', scatter_dimension=0, tiled=True)]
    all_gather x3 -> x0, waiting for transfers between devices: 109 us -> none  [the longest x2 63 us: shards(): current = lax.all_gather(share_rows, 'tp', axis=0, tiled=True)]
    pallas_call x0 -> x2, Pallas kernels: none -> 106 us  [the longest x1 103 us: shards(): pl.pallas_call(kernel, out_shape=jax.ShapeDtypeStruct((BLK, D), BF16), in...]
    dot_general x18 -> x0, matrix products: 56.7 us -> none  [the longest x3 15.4 us: project(): lax.dot_general(attended, out_weight, (((1,), (1,)), ((), ())), preferred...]
    reduce_sum x7 -> x0, other arithmetic: 18.4 us -> none  [the longest x4 10.9 us: norm_rows(): jnp.mean(wide_values * wide_values, axis=-1, keepdims=True) + EPS]
    ppermute x6 -> x0, starting transfers between devices: 14.2 us -> none  [the longest x3 10.2 us: extended_2(): lax.ppermute(lax.slice_in_dim(block, block.shape[dim] - width, None, axis...]
    convert_element_type x6 -> x0, other arithmetic: 9.17 us -> none  [the longest x3 5 us: shards(): normed = norm_rows(current, norm_gain[layer]).astype(jnp.bfloat16)]
    ppermute x6 -> x0, waiting for transfers between devices: 5.36 us -> none  [the longest x3 5.36 us: extended_2(): lax.ppermute(lax.slice_in_dim(block, 0, width, axis=dim), axis, backward)]
  transfers between devices with their start and end apart: 12 -> 0, of which waited for: 9 -> 0; matrix products, arithmetic and copies ran while one was open for 5% -> 0% of each run, Pallas kernels for 0% -> 0%
where the time goes in v2:
time: 108 us; the launch traced here: 106 us
  Pallas kernels  106 us (98%)
    pallas_call x1, Pallas kernels, shards(): pl.pallas_call(kernel, out_shape=jax.ShapeDtypeStruct((BLK, D), BF16), in...  103 us
    pallas_call x1, Pallas kernels, shards(): pl.pallas_call(last_norm, grid=(4,), out_shape=jax.ShapeDtypeStruct((BLK,...  3.49 us

profile of v2, /device:TPU:0, one launch (start us, length us, event | category | flops | bytes accessed | tf_op | source)
XLA Modules:
  0.0 106.1 jit_solution(4378721535195786758)
XLA Ops:
  0.0 102.6 %shard_map.82.rows = bf16[128,2048]{1,0:T(8,128)(2,1)} custom-call(bf16[1024,2048]{1,0:T(8,128)(2,1)} %inputs.1, bf16[3,128,128]{2,1,0:T(8,128)(2,1)} %q_w.1, bf16[3,64,128]{2,1,0:T(8,128)(2,1)} %bitcast.4, bf16[3,64,128]{2,1,0:T(8,128)(2,1)} %bitcast.5, bf16[3,128,128]{2,1,0:T(8,128)(2,1)} %o_w.1, f32[3,2048]{1,0:T(4,128)} %norm_gain_in.1, f32[2,3]{1,0:T(2,128)} %bitcast.7), custom_call_target="tpu_custom_call" | custom-call | tf_op jit(solution)/shard_map/pallas_call | solution.py:418
  102.6 3.5 %shard_map.83 = f32[128,2048]{1,0:T(8,128)} custom-call(bf16[128,2048]{1,0:T(8,128)(2,1)} %shard_map.82.rows, f32[1,2048]{1,0:T(1,128)} %bitcast.6), custom_call_target="tpu_custom_call" | custom-call | tf_op jit(solution)/shard_map/pallas_call | solution.py:450

commit v3 on v2

--- a/solution.py
+++ b/solution.py
@@ -23,7 +23,7 @@
 ROTATIONS = (("x", "y", "z"), ("y", "z", "x"), ("z", "x", "y"))
 DIMS = ("x", "z", "y")
 KV, Q, O = 0, 1, 2
-ROWS = (((0, 48), (48, 80), (80, 128)), ((0, 48), (48, 80), (80, 128)), ((0, 40), (40, 88), (88, 128)))
+ROWS = (((0, 48), (48, 96), (96, 128)), ((0, 48), (48, 80), (80, 128)), ((0, 32), (32, 80), (80, 128)))
 SPREADS = tuple((kind, lo, hi) for lo, hi in ((0, 1), (1, 3)) for kind in (KV, Q, O))
 GROUPS = tuple((kind, layer) for layer in range(LAYERS) for kind in (KV, Q, O))
 CHUNKS = 4
@@ -167,9 +167,9 @@
     def cube_in(g):
         landed(g, 3, 2, 4, 4)
 
-    def norm_rows(src, rows, write):
+    def norm_rows(src, first, rows, write):
         def body(i, carry):
-            at_row = pl.ds(pl.multiple_of(i * 16, 16), 16)
+            at_row = pl.ds(pl.multiple_of(first + i * 16, 16), 16)
             v = src(at_row)
             root = lax.rsqrt(jnp.mean(v * v, axis=-1, keepdims=True) + EPS)
             write(at_row, v * root)
@@ -254,27 +254,23 @@
     low_lane = lax.broadcasted_iota(jnp.int32, (BLK, BLK), 1) < HEAD_DIM
     low_key = lax.broadcasted_iota(jnp.int32, (3 * BLK, BLK), 1) < HEAD_DIM
 
-    def attention(l, lo, hi):
-        def body(h, carry):
-            for b in range(2):
-                kv = kv_rows[l, h, pl.ds(b * BLK, 3 * BLK)]
-                ones_v = jnp.where(low_key, jnp.ones_like(kv), kv)
-                s = lax.dot_general(q_rows[h, b], kv, (((1,), (1,)), ((), ())), preferred_element_type=F32)
-                sums, extra = [], []
-                for g in range(2):
-                    mine = s[g * BLK : (g + 1) * BLK] + bias[b]
-                    sink = sinks[h, pl.ds(2 * l + g, 1), pl.ds(0, 1)]
-                    m = jnp.maximum(jnp.max(mine, axis=1, keepdims=True), sink)
-                    p = jnp.exp2(mine - m).astype(BF16)
-                    sums.append(jnp.dot(p, ones_v, preferred_element_type=F32))
-                    extra.append(jnp.exp2(sink - m))
-                top = jnp.where(low_lane, pltpu.roll(sums[0], HEAD_DIM, 1), sums[1])
-                below = jnp.where(low_lane, sums[0], pltpu.roll(sums[1], HEAD_DIM, 1))
-                below = below + jnp.where(low_lane, extra[0], extra[1])
-                att[h, pl.ds(b * BLK, BLK)] = (top / below).astype(BF16)
-            return carry
-
-        lax.fori_loop(lo, hi, body, 0)
+    def attention(l, h):
+        for b in range(2):
+            kv = kv_rows[l, h, pl.ds(b * BLK, 3 * BLK)]
+            ones_v = jnp.where(low_key, jnp.ones_like(kv), kv)
+            s = lax.dot_general(q_rows[h, b], kv, (((1,), (1,)), ((), ())), preferred_element_type=F32)
+            sums, extra = [], []
+            for g in range(2):
+                mine = s[g * BLK : (g + 1) * BLK] + bias[b]
+                sink = sinks[h, pl.ds(2 * l + g, 1), pl.ds(0, 1)]
+                m = jnp.maximum(jnp.max(mine, axis=1, keepdims=True), sink)
+                p = jnp.exp2(mine - m).astype(BF16)
+                sums.append(jnp.dot(p, ones_v, preferred_element_type=F32))
+                extra.append(jnp.exp2(sink - m))
+            top = jnp.where(low_lane, pltpu.roll(sums[0], HEAD_DIM, 1), sums[1])
+            below = jnp.where(low_lane, sums[0], pltpu.roll(sums[1], HEAD_DIM, 1))
+            below = below + jnp.where(low_lane, extra[0], extra[1])
+            att[h, pl.ds(b * BLK, BLK)] = (top / below).astype(BF16)
 
     def part_rows(l, block):
         return pl.ds(pl.multiple_of(block * BLK, BLK), BLK) if l == LAYERS - 1 else slice(None)
@@ -286,122 +282,93 @@
             part_send.at[l, rows, cols], part_recv.at[l, rows, cols], part_ssem.at[l], part_rsem.at[l], peer
         ).start()
 
-    def project_out(l):
+    def project_out(l, j):
         lhs = jnp.concatenate([att[h] for h in range(RING)], axis=1)
-        for j in range(CHUNKS):
-
-            def body(i, carry):
-                pair = pl.ds(lax.rem(i, 2) * 2, 2)
-                w = jnp.concatenate(
-                    [w_all[l, h, i // 2, pair, pl.ds(O * BLK, BLK)].reshape(2 * BLK, BLK) for h in range(RING)],
-                    axis=1,
-                )
-                r = lax.dot_general(lhs, w, (((1,), (1,)), ((), ())), preferred_element_type=F32)
-                cols = pl.ds(pl.multiple_of(i * 2 * BLK, 2 * BLK), 2 * BLK)
-                part_own[:, cols] = r
-                part_send[l, :, cols] = r.astype(BF16)
-                return carry
-
-            lax.fori_loop(2 * j, 2 * j + 2, body, 0)
-            if j > 0:
-                send_part(l, j - 1)
+
+        def body(i, carry):
+            pair = pl.ds(lax.rem(i, 2) * 2, 2)
+            w = jnp.concatenate(
+                [w_all[l, h, i // 2, pair, pl.ds(O * BLK, BLK)].reshape(2 * BLK, BLK) for h in range(RING)],
+                axis=1,
+            )
+            r = lax.dot_general(lhs, w, (((1,), (1,)), ((), ())), preferred_element_type=F32)
+            cols = pl.ds(pl.multiple_of(i * 2 * BLK, 2 * BLK), 2 * BLK)
+            part_own[:, cols] = r
+            part_send[l, :, cols] = r.astype(BF16)
+            return carry
+
+        lax.fori_loop(2 * j, 2 * j + 2, body, 0)
+        if j > 0:
+            send_part(l, j - 1)
 
     def parts_in(l):
         all_in(part_recv.at[l, part_rows(l, c)], part_rsem.at[l])
 
-    def layer(l, steps):
-        project_kv(l)
-        steps[0]()
-        halo(l)
-        steps[1]()
-        project_q(l)
-        halo_in(l)
-        steps[2]()
-        attention(l, 0, 2)
-        steps[3]()
-        attention(l, 2, 4)
-        steps[4]()
-        project_out(l)
-        steps[5]()
+    def exchange(l):
         send_part(l, CHUNKS - 1)
         all_out(part_send.at[l, part_rows(l, 1 - c)], part_ssem.at[l])
         parts_in(l)
         if l == LAYERS - 1:
             mine = part_rows(l, c)
             out[...] = (part_own[mine] + part_recv[l, mine].astype(F32)).astype(BF16)
-            return
+
+    def norm_half(l, half):
+        gain = norm_gain[pl.ds(l + 1, 1)]
 
         def state(at_row):
             return (part_own[at_row] + part_recv[l, at_row].astype(F32)).astype(BF16).astype(F32)
 
-        gain = norm_gain[pl.ds(l + 1, 1)]
-
         def write_normed(at_row, v):
             normed[l + 1, at_row] = (v * gain).astype(BF16)
 
-        norm_rows(state, 2 * BLK, write_normed)
-        steps[6]()
-
-    def visits(*steps):
-        return [lambda calls=calls: [f(*a) for f, *a in calls] for calls in steps]
-
-    for i in range(3):
-        spread(i)
-    for copy in small:
-        copy.wait()
-    for l in range(LAYERS):
-        for g in range(2):
-            sink_tile[pl.ds(2 * l + g, 1)] = jnp.broadcast_to(sink_logit[pl.ds(g, 1), pl.ds(l, 1)], (1, BLK)) * LOG2E
-    sinks[x] = sink_tile[...]
-    for g in range(3):
-        spread_in(g)
-        plane(g)
-    for i in range(3, 6):
-        spread(i)
-    for i in range(1, RING):
-        remote(sink_tile, sinks.at[x], sink_sem.at[0], sink_sem.at[1], neighbour("x", i)).start()
-    all_out(sinks.at[0:3], sink_sem.at[0])
-    gain = norm_gain[pl.ds(0, 1)]
-
-    def write_first(at_row, v):
-        normed[0, at_row] = (v * gain).astype(BF16)
-
-    plane_on(0)
-    plane_on(1)
-    plane_in(0)
-    cube(0)
-    norm_rows(lambda at_row: staged[at_row].astype(F32), 2 * BLK, write_first)
-    plane_on(2)
-    spread_in(3)
-    plane(3)
-    plane_in(1)
-    cube(1)
-    make_bias()
-    cube_on(0)
-    spread_in(4)
-    plane(4)
-    plane_on(3)
-    plane_in(2)
-    cube(2)
-    make_tables()
-    spread_in(5)
-    plane(5)
-    plane_on(4)
-    all_in(sinks.at[0:3], sink_sem.at[1])
-    cube_in(0)
-    last = len(GROUPS) - 1
-    for l in range(LAYERS):
-        g = 3 * l
-        plan = (
-            [],
-            [(cube_on, 1), (plane_in, 3), (cube, 3), (cube_on, 2), (plane_on, 5), (plane, 6), (cube_in, 1)],
-            [(plane_on, 6), (plane, 7), (plane_in, 4), (cube, 4)],
-            [(cube_on, 3)],
-            [(cube_in, 2)],
-            [(plane_on, 7), (plane, 8), (plane_in, 5), (cube, 5)],
-            [(cube_in, 3)],
-        )
-        layer(l, visits(*([(f, g + n) for f, n in step if g + n <= last] for step in plan)))
+        norm_rows(state, half * BLK, BLK, write_normed)
+
+    def first_norm(half):
+        gain = norm_gain[pl.ds(0, 1)]
+
+        def write_first(at_row, v):
+            normed[0, at_row] = (v * gain).astype(BF16)
+
+        norm_rows(lambda at_row: staged[at_row].astype(F32), half * BLK, BLK, write_first)
+
+    def share_sinks():
+        for copy in small:
+            copy.wait()
+        for l in range(LAYERS):
+            for g in range(2):
+                sink = jnp.broadcast_to(sink_logit[pl.ds(g, 1), pl.ds(l, 1)], (1, BLK))
+                sink_tile[pl.ds(2 * l + g, 1)] = sink * LOG2E
+        sinks[x] = sink_tile[...]
+        for i in range(1, RING):
+            remote(sink_tile, sinks.at[x], sink_sem.at[0], sink_sem.at[1], neighbour("x", i)).start()
+        all_out(sinks.at[0:3], sink_sem.at[0])
+
+    def sinks_in():
+        all_in(sinks.at[0:3], sink_sem.at[1])
+
+    order = (
+        (spread, 0), (spread, 2), (spread, 5), (make_tables,), (spread, 4), (spread, 1), (share_sinks,),
+        (spread_in, 0), (plane, 0), (spread, 3), (spread_in, 2), (spread_in, 5), (plane, 5), (spread_in, 4),
+        (make_bias,), (plane, 4), (plane_on, 0), (plane, 2), (spread_in, 1), (plane, 1), (first_norm, 0),
+        (spread_in, 3), (plane_on, 5), (plane, 3), (plane_in, 0), (plane_on, 4), (plane_on, 2), (cube, 0),
+        (plane_on, 1), (plane_on, 3), (first_norm, 1), (plane, 6), (plane_in, 2), (cube_on, 0), (cube, 2),
+        (plane_in, 1), (plane_in, 5), (cube_in, 0), (cube, 1), (plane_in, 4), (project_kv, 0), (halo, 0),
+        (cube_on, 1), (plane_in, 3), (cube_on, 2), (plane, 8), (cube, 3), (cube_in, 1), (plane_on, 6),
+        (cube, 4), (sinks_in,), (halo_in, 0), (project_q, 0), (attention, 0, 0), (attention, 0, 1),
+        (cube_on, 3), (attention, 0, 2), (attention, 0, 3), (cube_in, 2), (project_out, 0, 0),
+        (project_out, 0, 1), (cube_on, 4), (project_out, 0, 2), (cube, 5), (plane, 7), (project_out, 0, 3),
+        (exchange, 0), (plane_in, 6), (norm_half, 0, 0), (norm_half, 0, 1), (cube_in, 3), (project_kv, 1),
+        (cube_in, 4), (halo, 1), (plane_on, 7), (cube_on, 5), (project_q, 1), (cube, 6), (halo_in, 1),
+        (plane_on, 8), (attention, 1, 0), (plane_in, 7), (attention, 1, 1), (cube_on, 6), (attention, 1, 2),
+        (cube_in, 5), (cube, 7), (attention, 1, 3), (project_out, 1, 0), (project_out, 1, 1),
+        (project_out, 1, 2), (project_out, 1, 3), (exchange, 1), (cube_in, 6), (plane_in, 8),
+        (norm_half, 1, 0), (cube_on, 7), (norm_half, 1, 1), (project_kv, 2), (halo, 2), (cube, 8),
+        (cube_in, 7), (project_q, 2), (cube_on, 8), (halo_in, 2), (attention, 2, 0), (attention, 2, 1),
+        (attention, 2, 2), (attention, 2, 3), (cube_in, 8), (project_out, 2, 0), (project_out, 2, 1),
+        (project_out, 2, 2), (project_out, 2, 3), (exchange, 2),
+    )
+    for step, *arguments in order:
+        step(*arguments)
     for copy in unsent:
         copy.wait_send()
 

time: 108 us -> 101 us (0.935)
  Pallas kernels: 106 us -> 99.5 us
    pallas_call x1, Pallas kernels: 103 us -> 96 us  [shards(): pl.pallas_call(kernel, out_shape=jax.ShapeDtypeStruct((BLK, D), BF16), in...]
where the time goes in v3:
time: 101 us; the launch traced here: 99.5 us
  Pallas kernels  99.5 us (99%)
    pallas_call x1, Pallas kernels, shards(): pl.pallas_call(kernel, out_shape=jax.ShapeDtypeStruct((BLK, D), BF16), in...  96 us
    pallas_call x1, Pallas kernels, shards(): pl.pallas_call(last_norm, grid=(4,), out_shape=jax.ShapeDtypeStruct((BLK,...  3.49 us

profile of v3, /device:TPU:0, one launch (start us, length us, event | category | flops | bytes accessed | tf_op | source)
XLA Modules:
  0.0 99.5 jit_solution(13046272358724813758)
XLA Ops:
  0.0 96.0 %shard_map.82.rows = bf16[128,2048]{1,0:T(8,128)(2,1)} custom-call(bf16[1024,2048]{1,0:T(8,128)(2,1)} %inputs.1, bf16[3,128,128]{2,1,0:T(8,128)(2,1)} %q_w.1, bf16[3,64,128]{2,1,0:T(8,128)(2,1)} %bitcast.4, bf16[3,64,128]{2,1,0:T(8,128)(2,1)} %bitcast.5, bf16[3,128,128]{2,1,0:T(8,128)(2,1)} %o_w.1, f32[3,2048]{1,0:T(4,128)} %norm_gain_in.1, f32[2,3]{1,0:T(2,128)} %bitcast.7), custom_call_target="tpu_custom_call" | custom-call | tf_op jit(solution)/shard_map/pallas_call | solution.py:385
  96.0 3.5 %shard_map.83 = f32[128,2048]{1,0:T(8,128)} custom-call(bf16[128,2048]{1,0:T(8,128)(2,1)} %shard_map.82.rows, f32[1,2048]{1,0:T(1,128)} %bitcast.6), custom_call_target="tpu_custom_call" | custom-call | tf_op jit(solution)/shard_map/pallas_call | solution.py:417

commit v4 on v3

--- a/solution.py
+++ b/solution.py
@@ -154,6 +154,8 @@
     def cube(g):
         hop(g, 2, 0, 0, 2, 1)
         hop(g, 2, 0, 1, 2, -1)
+
+    def cube_more(g):
         hop(g, 2, 0, 1, 3, 1)
         hop(g, 2, 0, 0, 3, -1)
 
@@ -347,25 +349,26 @@
         all_in(sinks.at[0:3], sink_sem.at[1])
 
     order = (
-        (spread, 0), (spread, 2), (spread, 5), (make_tables,), (spread, 4), (spread, 1), (share_sinks,),
-        (spread_in, 0), (plane, 0), (spread, 3), (spread_in, 2), (spread_in, 5), (plane, 5), (spread_in, 4),
-        (make_bias,), (plane, 4), (plane_on, 0), (plane, 2), (spread_in, 1), (plane, 1), (first_norm, 0),
-        (spread_in, 3), (plane_on, 5), (plane, 3), (plane_in, 0), (plane_on, 4), (plane_on, 2), (cube, 0),
-        (plane_on, 1), (plane_on, 3), (first_norm, 1), (plane, 6), (plane_in, 2), (cube_on, 0), (cube, 2),
-        (plane_in, 1), (plane_in, 5), (cube_in, 0), (cube, 1), (plane_in, 4), (project_kv, 0), (halo, 0),
-        (cube_on, 1), (plane_in, 3), (cube_on, 2), (plane, 8), (cube, 3), (cube_in, 1), (plane_on, 6),
-        (cube, 4), (sinks_in,), (halo_in, 0), (project_q, 0), (attention, 0, 0), (attention, 0, 1),
-        (cube_on, 3), (attention, 0, 2), (attention, 0, 3), (cube_in, 2), (project_out, 0, 0),
-        (project_out, 0, 1), (cube_on, 4), (project_out, 0, 2), (cube, 5), (plane, 7), (project_out, 0, 3),
+        (spread, 1), (spread, 0), (make_bias,), (spread, 2), (spread, 3), (share_sinks,), (first_norm, 0),
+        (spread, 5), (spread, 4), (spread_in, 1), (plane, 1), (spread_in, 2), (plane, 2), (spread_in, 0),
+        (spread_in, 3), (plane, 0), (spread_in, 5), (plane, 3), (plane, 6), (plane, 5), (plane_on, 0),
+        (spread_in, 4), (plane, 4), (make_tables,), (plane_on, 1), (plane, 8), (plane_on, 3), (plane_on, 2),
+        (plane_in, 0), (cube, 0), (cube_more, 0), (plane_on, 6), (plane_on, 8), (first_norm, 1), (plane_on, 4),
+        (plane_in, 1), (plane_in, 2), (plane_on, 5), (cube_on, 0), (cube, 1), (cube, 2), (cube_more, 1),
+        (plane_in, 5), (plane_in, 3), (cube_in, 0), (project_kv, 0), (halo, 0), (cube_on, 1), (cube, 3),
+        (cube_more, 2), (cube_on, 2), (plane_in, 4), (cube_in, 1), (cube, 4), (cube_more, 3), (project_q, 0),
+        (cube_on, 3), (sinks_in,), (halo_in, 0), (cube_more, 4), (plane, 7), (cube, 5), (attention, 0, 0),
+        (attention, 0, 1), (attention, 0, 2), (cube_in, 2), (attention, 0, 3), (project_out, 0, 0),
+        (project_out, 0, 1), (project_out, 0, 2), (project_out, 0, 3), (plane_in, 8), (cube_on, 4),
         (exchange, 0), (plane_in, 6), (norm_half, 0, 0), (norm_half, 0, 1), (cube_in, 3), (project_kv, 1),
-        (cube_in, 4), (halo, 1), (plane_on, 7), (cube_on, 5), (project_q, 1), (cube, 6), (halo_in, 1),
-        (plane_on, 8), (attention, 1, 0), (plane_in, 7), (attention, 1, 1), (cube_on, 6), (attention, 1, 2),
-        (cube_in, 5), (cube, 7), (attention, 1, 3), (project_out, 1, 0), (project_out, 1, 1),
-        (project_out, 1, 2), (project_out, 1, 3), (exchange, 1), (cube_in, 6), (plane_in, 8),
-        (norm_half, 1, 0), (cube_on, 7), (norm_half, 1, 1), (project_kv, 2), (halo, 2), (cube, 8),
-        (cube_in, 7), (project_q, 2), (cube_on, 8), (halo_in, 2), (attention, 2, 0), (attention, 2, 1),
-        (attention, 2, 2), (attention, 2, 3), (cube_in, 8), (project_out, 2, 0), (project_out, 2, 1),
-        (project_out, 2, 2), (project_out, 2, 3), (exchange, 2),
+        (halo, 1), (plane_on, 7), (cube, 6), (cube_more, 5), (cube_on, 5), (plane_in, 7), (cube, 7),
+        (cube_in, 4), (project_q, 1), (halo_in, 1), (cube_more, 6), (attention, 1, 0), (cube_on, 6),
+        (attention, 1, 1), (attention, 1, 2), (cube_more, 7), (cube_in, 5), (attention, 1, 3), (cube_on, 7),
+        (project_out, 1, 0), (project_out, 1, 1), (project_out, 1, 2), (project_out, 1, 3), (exchange, 1),
+        (norm_half, 1, 0), (cube_in, 6), (cube, 8), (norm_half, 1, 1), (project_kv, 2), (halo, 2),
+        (cube_more, 8), (cube_in, 7), (project_q, 2), (cube_on, 8), (halo_in, 2), (attention, 2, 0),
+        (cube_in, 8), (attention, 2, 1), (attention, 2, 2), (attention, 2, 3), (project_out, 2, 0),
+        (project_out, 2, 1), (project_out, 2, 2), (project_out, 2, 3), (exchange, 2),
     )
     for step, *arguments in order:
         step(*arguments)
@@ -373,9 +376,16 @@
         copy.wait_send()
 
 
-def last_norm(rows, gain, out):
-    v = rows[...].astype(F32)
-    out[...] = v * lax.rsqrt(jnp.mean(v * v, axis=-1, keepdims=True) + EPS) * gain[...]
+def last_norm(rows, gain, out, done, sems):
+    copies = []
+    for i in range(4):
+        part = pl.ds(i * 32, 32)
+        v = rows[part].astype(F32)
+        done[part] = v * lax.rsqrt(jnp.mean(v * v, axis=-1, keepdims=True) + EPS) * gain[...]
+        copies.append(pltpu.make_async_copy(done.at[part], out.at[part], sems.at[i]))
+        copies[-1].start()
+    for copy in copies:
+        copy.wait()
 
 
 def shards(inputs, norm_gain, query_weight, key_weight, value_weight, output_weight, sink_logit, final_gain):
@@ -407,19 +417,19 @@
             dma((7,)), dma((LAYERS,)), dma((LAYERS,)), dma((LAYERS,)), dma((LAYERS,)), dma((2,)),
         ],
         compiler_params=pltpu.CompilerParams(
-            collective_id=0, has_side_effects=True, vmem_limit_bytes=67043328
+            collective_id=0, has_side_effects=True, vmem_limit_bytes=66400000
         ),
     )(
         inputs, query_weight, jnp.swapaxes(key_weight, 1, 2), jnp.swapaxes(value_weight, 1, 2), output_weight,
         norm_gain, jnp.swapaxes(sink_logit, 0, 1),
     )
-    step = BLK // 4
     return pl.pallas_call(
         last_norm,
-        grid=(4,),
         out_shape=jax.ShapeDtypeStruct((BLK, D), F32),
-        in_specs=[pl.BlockSpec((step, D), lambda i: (i, 0)), pl.BlockSpec((1, D), lambda i: (0, 0))],
-        out_specs=pl.BlockSpec((step, D), lambda i: (i, 0)),
+        in_specs=[vmem, vmem],
+        out_specs=hbm,
+        scratch_shapes=[pltpu.VMEM((BLK, D), F32), dma((4,))],
+        compiler_params=pltpu.CompilerParams(vmem_limit_bytes=8 * 1024 * 1024),
     )(rows, final_gain.reshape(1, D))
 
 

time: 101 us -> 97.3 us (0.963)
  Pallas kernels: 99.5 us -> 94.6 us
  local copies, waits for them, and re-layouts: 0 us -> 1.04 us
    pallas_call x1, Pallas kernels: 96 us -> 93.4 us  [shards(): pl.pallas_call(kernel, out_shape=jax.ShapeDtypeStruct((BLK, D), BF16), in...]
    pallas_call x1, Pallas kernels: 3.49 us -> 1.12 us  [shards(): pl.pallas_call(last_norm, out_shape=jax.ShapeDtypeStruct((BLK, D), F32),...]
    unnamed x0 -> x4, local copies, waits for them, and re-layouts: none -> 1.04 us
where the time goes in v4:
time: 97.3 us; the launch traced here: 95.8 us
  Pallas kernels  94.6 us (97%)
  local copies, waits for them, and re-layouts  1.04 us (1%)
    pallas_call x1, Pallas kernels, shards(): pl.pallas_call(kernel, out_shape=jax.ShapeDtypeStruct((BLK, D), BF16), in...  93.4 us

profile of v4, /device:TPU:0, one launch (start us, length us, event | category | flops | bytes accessed | tf_op | source)
XLA Modules:
  0.0 95.8 jit_solution(13690963597922541191)
XLA Ops:
  0.0 0.0 copy-start.1
  0.0 93.4 %shard_map.82.rows = bf16[128,2048]{1,0:T(8,128)(2,1)} custom-call(bf16[1024,2048]{1,0:T(8,128)(2,1)} %inputs.1, bf16[3,128,128]{2,1,0:T(8,128)(2,1)} %q_w.1, bf16[3,64,128]{2,1,0:T(8,128)(2,1)} %bitcast.5, bf16[3,64,128]{2,1,0:T(8,128)(2,1)} %bitcast.6, bf16[3,128,128]{2,1,0:T(8,128)(2,1)} %o_w.1, f32[3,2048]{1,0:T(4,128)} %norm_gain_in.1, f32[2,3]{1,0:T(2,128)} %bitcast.7), custom_call_target="tpu_custom_call" | custom-call | tf_op jit(solution)/shard_map/pallas_call | solution.py:395
  93.5 0.0 copy-done.1
  93.5 0.0 copy-start
  93.5 1.0 %copy-done = bf16[128,2048]{1,0:T(8,128)(2,1)S(1)} copy-done((bf16[128,2048]{1,0:T(8,128)(2,1)S(1)}, bf16[128,2048]{1,0:T(8,128)(2,1)}, u32[]{:S(2)}) %copy-start) | copy-done | bytes 524312
  94.5 1.1 %shard_map.83 = f32[128,2048]{1,0:T(8,128)} custom-call(bf16[128,2048]{1,0:T(8,128)(2,1)S(1)} %copy-done, f32[1,2048]{1,0:T(1,128)S(1)} %bitcast.4), custom_call_target="tpu_custom_call" | custom-call | tf_op jit(solution)/shard_map/pallas_call | solution.py:426
Async XLA Ops:
  0.0 93.5 %copy-start.1 = (f32[2048]{0:T(1024)S(1)}, f32[2048]{0:T(1024)}, u32[]{:S(2)}) copy-start(f32[2048]{0:T(1024)} %param.15) | copy-start | bytes 24580
  93.5 1.0 %copy-start = (bf16[128,2048]{1,0:T(8,128)(2,1)S(1)}, bf16[128,2048]{1,0:T(8,128)(2,1)}, u32[]{:S(2)}) copy-start(bf16[128,2048]{1,0:T(8,128)(2,1)} %shard_map.82.rows) | copy-start | bytes 1572868

commit v5 on v4

--- a/solution.py
+++ b/solution.py
@@ -223,7 +223,8 @@
                 kv_rows[l, 2 * i + j, pl.ds(BLK, 2 * BLK)] = kv.astype(BF16)
             return carry
 
-        lax.fori_loop(0, 2, body, 0)
+        for i in range(2):
+            body(i, 0)
 
     def project_q(l):
         def body(i, carry):
@@ -240,7 +241,8 @@
                     q_rows[2 * i + j, b, pl.ds(BLK, BLK)] = head1[b * BLK : (b + 1) * BLK]
             return carry
 
-        lax.fori_loop(0, 2, body, 0)
+        for i in range(2):
+            body(i, 0)
 
     def halo(l):
         rows = kv_rows.at[l]
@@ -288,18 +290,19 @@
         lhs = jnp.concatenate([att[h] for h in range(RING)], axis=1)
 
         def body(i, carry):
-            pair = pl.ds(lax.rem(i, 2) * 2, 2)
+            pair = pl.ds(i % 2 * 2, 2)
             w = jnp.concatenate(
                 [w_all[l, h, i // 2, pair, pl.ds(O * BLK, BLK)].reshape(2 * BLK, BLK) for h in range(RING)],
                 axis=1,
             )
             r = lax.dot_general(lhs, w, (((1,), (1,)), ((), ())), preferred_element_type=F32)
-            cols = pl.ds(pl.multiple_of(i * 2 * BLK, 2 * BLK), 2 * BLK)
+            cols = pl.ds(i * 2 * BLK, 2 * BLK)
             part_own[:, cols] = r
             part_send[l, :, cols] = r.astype(BF16)
             return carry
 
-        lax.fori_loop(2 * j, 2 * j + 2, body, 0)
+        for i in (2 * j, 2 * j + 1):
+            body(i, 0)
         if j > 0:
             send_part(l, j - 1)
 

time: 97.3 us -> 96 us (0.987)
  Pallas kernels: 94.6 us -> 93.2 us
    pallas_call x1, Pallas kernels: 93.4 us -> 92.1 us  [shards(): pl.pallas_call(kernel, out_shape=jax.ShapeDtypeStruct((BLK, D), BF16), in...]
where the time goes in v5:
time: 96 us; the launch traced here: 94.4 us
  Pallas kernels  93.2 us (97%)
  local copies, waits for them, and re-layouts  1.04 us (1%)
    pallas_call x1, Pallas kernels, shards(): pl.pallas_call(kernel, out_shape=jax.ShapeDtypeStruct((BLK, D), BF16), in...  92.1 us

profile of v5, /device:TPU:0, one launch (start us, length us, event | category | flops | bytes accessed | tf_op | source)
XLA Modules:
  0.0 94.4 jit_solution(6503572538814775020)
XLA Ops:
  0.0 0.0 copy-start.1
  0.0 92.1 %shard_map.82.rows = bf16[128,2048]{1,0:T(8,128)(2,1)} custom-call(bf16[1024,2048]{1,0:T(8,128)(2,1)} %inputs.1, bf16[3,128,128]{2,1,0:T(8,128)(2,1)} %q_w.1, bf16[3,64,128]{2,1,0:T(8,128)(2,1)} %bitcast.5, bf16[3,64,128]{2,1,0:T(8,128)(2,1)} %bitcast.6, bf16[3,128,128]{2,1,0:T(8,128)(2,1)} %o_w.1, f32[3,2048]{1,0:T(4,128)} %norm_gain_in.1, f32[2,3]{1,0:T(2,128)} %bitcast.7), custom_call_target="tpu_custom_call" | custom-call | tf_op jit(solution)/shard_map/pallas_call | solution.py:398
  92.1 0.0 copy-done.1
  92.1 0.0 copy-start
  92.1 1.0 %copy-done = bf16[128,2048]{1,0:T(8,128)(2,1)S(1)} copy-done((bf16[128,2048]{1,0:T(8,128)(2,1)S(1)}, bf16[128,2048]{1,0:T(8,128)(2,1)}, u32[]{:S(2)}) %copy-start) | copy-done | bytes 524312
  93.1 1.1 %shard_map.83 = f32[128,2048]{1,0:T(8,128)} custom-call(bf16[128,2048]{1,0:T(8,128)(2,1)S(1)} %copy-done, f32[1,2048]{1,0:T(1,128)S(1)} %bitcast.4), custom_call_target="tpu_custom_call" | custom-call | tf_op jit(solution)/shard_map/pallas_call | solution.py:429
Async XLA Ops:
  0.0 92.1 %copy-start.1 = (f32[2048]{0:T(1024)S(1)}, f32[2048]{0:T(1024)}, u32[]{:S(2)}) copy-start(f32[2048]{0:T(1024)} %param.15) | copy-start | bytes 24580
  92.1 1.0 %copy-start = (bf16[128,2048]{1,0:T(8,128)(2,1)S(1)}, bf16[128,2048]{1,0:T(8,128)(2,1)}, u32[]{:S(2)}) copy-start(bf16[128,2048]{1,0:T(8,128)(2,1)} %shard_map.82.rows) | copy-start | bytes 1572868
